TPU v7x, 256 devices: a whole 4x4x8 slice. The times are simulated.
256 devices in a mesh: fs: 64 (over z, x, core), tp: 4 (over y).
Axes of the slice: x: 4, y: 4, z: 8, core: 2. Of those that a mesh axis runs over, the one named last changes fastest.
Arguments:
- x_late: bfloat16 [32768, 2048], P(('fs', 'tp')), may hold values from -6 to 6
- x_early: bfloat16 [32768, 2048], P(('fs', 'tp')), may hold values from -24 to 24
- d_hidden: bfloat16 [32768, 3072], P('fs', 'tp'), may hold values from -16 to 16
- w_gate: bfloat16 [2048, 3072], P('fs', 'tp'), may hold values from -0.125 to 0.125
- w_up: bfloat16 [2048, 3072], P('fs', 'tp'), may hold values from -0.125 to 0.125
- gate_sum: float32 [2048, 3072], P('fs', 'tp'), may hold values from -512 to 512
- up_sum: float32 [2048, 3072], P('fs', 'tp'), may hold values from -512 to 512
Outputs:
- hidden_late: bfloat16 [32768, 3072], P('fs', 'tp')
- grad_input: bfloat16 [32768, 2048], P(('fs', 'tp'))
- gate_sum_out: float32 [2048, 3072], P('fs', 'tp')
- up_sum_out: float32 [2048, 3072], P('fs', 'tp')
All inputs are finite; a program needn't handle non-finite values.
Results may differ from a plain program's by a relative error of at most 0.0095.
Values may be sent and summed in bfloat16 or wider, within the bound.
A program may use at most 128 MiB of HBM per device.

v0:
```python
import jax
import jax.numpy as jnp
from jax import lax
from jax.sharding import PartitionSpec as P


def from_everyone(x, axis):
    copies = jnp.broadcast_to(x, (lax.axis_size(axis), *x.shape))
    return lax.all_to_all(copies, axis, split_axis=0, concat_axis=0, tiled=True)


def joined_along(pieces, dim):
    pieces = jnp.moveaxis(pieces, 0, dim)
    dims = pieces.shape
    return pieces.reshape(*dims[:dim], dims[dim] * dims[dim + 1], *dims[dim + 2 :])


def gather_directly(x, axis, dim):
    pieces = from_everyone(x, axis)
    return joined_along(pieces, dim)


def sent_together(arrays, axis, dim, along):
    widths = [a.shape[along] for a in arrays]
    both = jnp.concatenate(arrays, axis=along)
    result = lax.all_gather(both, axis, axis=dim, tiled=True)
    return tuple(jnp.split(result, [sum(widths[:k]) for k in range(1, len(widths))], axis=along))


def in_blocks(x, dim, devices):
    before, after = (x.shape[:dim], x.shape[dim + 1 :])
    return jnp.moveaxis(x.reshape(*before, devices, -1, *after), dim, 0)


def summed_on_arrival(x, axis, dim):
    devices = lax.axis_size(axis)
    pieces = lax.all_to_all(in_blocks(x, dim, devices), axis, 0, 0, tiled=True)
    return jnp.sum(pieces.astype(jnp.float32), axis=0)


def local(x_late, x_early, d_hidden, w_gate, w_up, gate_sum, up_sum):
    rows_late = gather_directly(x_late, "tp", 0)
    rows_early = gather_directly(x_early, "tp", 0)
    stacked = jnp.concatenate([rows_late, rows_early], axis=0)
    row_count = rows_late.shape[0]
    col_count = w_gate.shape[1]
    contract = (((1,), (1,)), ((), ()))
    tokens_dim = (((0,), (0,)), ((), ()))
    full_gate, full_up = sent_together((w_gate, w_up), "fs", 0, 1)
    gate_pre = jnp.dot(stacked, full_gate, preferred_element_type=jnp.float32)
    up_pre = jnp.dot(stacked, full_up, preferred_element_type=jnp.float32)
    sigmoid_all = jax.nn.sigmoid(gate_pre)
    hidden_late = (gate_pre[:row_count] * sigmoid_all[:row_count] * up_pre[:row_count]).astype(
        jnp.bfloat16
    )
    gate_early = gate_pre[row_count:]
    up_early = up_pre[row_count:]
    sigmoid_early = sigmoid_all[row_count:]
    cotangent = d_hidden.astype(jnp.float32)
    d_gate = (
        cotangent * up_early * sigmoid_early * (1.0 + gate_early * (1.0 - sigmoid_early))
    ).astype(jnp.bfloat16)
    d_up = (cotangent * gate_early * sigmoid_early).astype(jnp.bfloat16)
    full_gate, full_up = sent_together((w_gate, w_up), "fs", 0, 1)
    partial_value = lax.dot_general(d_gate, full_gate, contract, preferred_element_type=jnp.float32)
    partial_value = partial_value + lax.dot_general(
        d_up, full_up, contract, preferred_element_type=jnp.float32
    )
    rounded = lax.optimization_barrier(partial_value.astype(jnp.bfloat16)).astype(jnp.float32)
    grad_input = summed_on_arrival(rounded.astype(jnp.bfloat16), "tp", 0).astype(jnp.bfloat16)
    d_both = jnp.concatenate([d_gate, d_up], axis=1)
    gradient = lax.psum_scatter(
        lax.dot_general(rows_early, d_both, tokens_dim, preferred_element_type=jnp.float32),
        "fs",
        scatter_dimension=0,
        tiled=True,
    )
    gate_grad = gradient[:, :col_count]
    up_grad = gradient[:, col_count:]
    return (hidden_late, grad_input, gate_sum + gate_grad, up_sum + up_grad)


def solution(mesh):
    return jax.shard_map(
        local,
        mesh=mesh,
        in_specs=(
            P(("fs", "tp"), None),
            P(("fs", "tp"), None),
            P("fs", "tp"),
            P("fs", "tp"),
            P("fs", "tp"),
            P("fs", "tp"),
            P("fs", "tp"),
        ),
        out_specs=(P("fs", "tp"), P(("fs", "tp"), None), P("fs", "tp"), P("fs", "tp")),
        check_vma=False,
    )
```

profile of v0, /device:TPU:2, one launch (start us, length us, event | category | flops | bytes accessed | tf_op | source)
XLA Modules:
  0.0 295.9 jit_solution(14229169420221778254)
XLA Ops:
  7.2 0.0 all-gather.2.cloned.1.call-start
  7.2 1.5 pad_maximum_fusion.3
  8.7 1.3 broadcast_in_dim.7
  10.1 30.6 %all_to_all.15 = bf16[4,128,2048]{2,1,0:T(8,128)(2,1)S(1)} all-to-all(bf16[4,128,2048]{2,1,0:T(8,128)(2,1)S(1)} %broadcast_in_dim.7), channel_id=1, replica_groups=mesh['fs'=64,'tp'=4] {'tp'}, dimensions={0} | all-to-all | bytes 4194304 | tf_op jit(solution)/shard_map/all_to_all | solution.py:9
  40.7 1.8 broadcast_in_dim.6
  42.4 4.5 %all-to-all-start = ((bf16[4,128,2048]{2,1,0:T(8,128)(2,1)}), bf16[4,128,2048]{2,1,0:T(8,128)(2,1)}, u32[]{:S(2)}, u32[]{:S(2)}) async-start(bf16[4,128,2048]{2,1,0:T(8,128)(2,1)} %broadcast_in_dim.6), calls=%async_computation | async-start | bytes 4194304 | tf_op jit(solution)/shard_map/all_to_all | solution.py:9
  46.9 0.0 reduce-scatter.4.cloned.1.call-start
  47.0 1.4 copy.17
  48.4 24.1 %all-to-all-done = bf16[4,128,2048]{2,1,0:T(8,128)(2,1)} async-done(((bf16[4,128,2048]{2,1,0:T(8,128)(2,1)}), bf16[4,128,2048]{2,1,0:T(8,128)(2,1)}, u32[]{:S(2)}, u32[]{:S(2)}) %all-to-all-start) | async-done | bytes 2097184 | tf_op jit(solution)/shard_map/all_to_all | solution.py:9
  72.5 21.1 %all-gather.2.cloned.1.call-done = bf16[2048,1536]{1,0:T(8,128)(2,1)} async-done(((bf16[32,1536]{1,0:T(8,128)(2,1)}), bf16[2048,1536]{1,0:T(8,128)(2,1)}) %all-gather.2.cloned.1.call-update) | async-done | bytes 6291472 | tf_op jit(solution)/shard_map/all_gather | solution.py:26
  93.6 6.6 %add_divide_fusion = (f32[1024,768]{0,1:T(8,128)S(1)}, f32[1024,768]{0,1:T(8,128)S(1)}) fusion(bf16[2048,1536]{1,0:T(8,128)(2,1)} %all-gather.2.cloned.1.call-done, bf16[512,2048]{1,0:T(8,128)(2,1)S(1)} %bitcast.9, bf16[512,2048]{1,0:T(8,128)(2,1)} %bitcast), kind=kOutput, calls=%fused_computation.3 | convolution fusion | flops 3231973376 | bytes 13631488 | tf_op jit(solution)/shard_map/dot_general | solution.py:50
  100.2 5.2 %fusion.1 = f32[1024,768]{0,1:T(8,128)S(1)} fusion(bf16[2048,1536]{1,0:T(8,128)(2,1)S(1)} %copy-done.8, bf16[512,2048]{1,0:T(8,128)(2,1)S(1)} %bitcast.10, bf16[512,2048]{1,0:T(8,128)(2,1)} %bitcast), kind=kOutput, calls=%fused_computation.5 | convolution fusion | flops 3229614080 | bytes 10485760 | tf_op jit(solution)/shard_map/dot_general | solution.py:51
  105.4 1.3 fusion.9
  106.8 0.9 copy-done.3
  107.7 7.3 %convolution_bitcast_fusion = f32[2048,1536]{0,1:T(8,128)} fusion(bf16[512,2048]{1,0:T(8,128)(2,1)S(1)} %bitcast.11, bf16[512,768]{0,1:T(8,128)(2,1)S(1)} %get-tuple-element.14, bf16[512,768]{0,1:T(8,128)(2,1)S(1)} %get-tuple-element.12), kind=kOutput, calls=%fused_computation | convolution fusion | flops 3224371200 | bytes 16252928 | tf_op jit(solution)/shard_map/dot_general | solution.py:73
  115.0 12.6 %copy.23 = f32[2048,1536]{1,0:T(8,128)} copy(f32[2048,1536]{0,1:T(8,128)} %convolution_bitcast_fusion) | data formatting | bytes 25165824
  127.6 0.0 reduce-scatter.4.cloned.1.call-update
  127.6 1.1 copy-done.4
  128.7 3.7 %fusion.3 = f32[512,2048]{1,0:T(8,128)S(1)} fusion(bf16[512,768]{0,1:T(8,128)(2,1)S(1)} %copy-done.4, bf16[2048,1536]{1,0:T(8,128)(2,1)} %all-gather.2.cloned.1.call-done), kind=kOutput, calls=%fused_computation.7 | convolution fusion | flops 1610612736 | bytes 8126464 | tf_op jit(solution)/shard_map/dot_general | solution.py:65
  132.5 5.2 %add_convert_fusion = bf16[512,2048]{1,0:T(8,128)(2,1)} fusion(f32[512,2048]{1,0:T(8,128)S(1)} %fusion.3, bf16[512,768]{0,1:T(8,128)(2,1)S(1)} %get-tuple-element.14, bf16[2048,1536]{1,0:T(8,128)(2,1)} %all-gather.2.cloned.1.call-done), kind=kOutput, calls=%fused_computation.2 | convolution fusion | flops 1612709888 | bytes 10223616 | tf_op jit(solution)/shard_map/dot_general | solution.py:66
  137.6 4.4 %all-to-all-start.2 = ((bf16[4,128,2048]{2,1,0:T(8,128)(2,1)}), bf16[4,128,2048]{2,1,0:T(8,128)(2,1)S(1)}, u32[]{:S(2)}, u32[]{:S(2)}) async-start(bf16[4,128,2048]{2,1,0:T(8,128)(2,1)} %bitcast.12), calls=%async_computation.2 | async-start | bytes 4194304 | tf_op jit(solution)/shard_map/all_to_all | solution.py:37
  142.0 0.9 copy.19
  142.9 0.2 copy.18
  143.1 1.2 copy.20
  144.3 24.5 %all-to-all-done.2 = bf16[4,128,2048]{2,1,0:T(8,128)(2,1)S(1)} async-done(((bf16[4,128,2048]{2,1,0:T(8,128)(2,1)}), bf16[4,128,2048]{2,1,0:T(8,128)(2,1)S(1)}, u32[]{:S(2)}, u32[]{:S(2)}) %all-to-all-start.2) | async-done | bytes 2097184 | tf_op jit(solution)/shard_map/all_to_all | solution.py:37
  168.8 1.3 reduce_sum.12
  170.1 116.1 %reduce-scatter.4.cloned.1.call-done = f32[32,1536]{1,0:T(8,128)} async-done(((f32[2048,1536]{1,0:T(8,128)}), f32[32,1536]{1,0:T(8,128)}) %reduce-scatter.4.cloned.1.call-update) | async-done | bytes 196624
  286.1 1.0 fusion.19
  287.1 0.2 copy.26
  287.3 0.8 copy.22
  288.1 0.2 copy.25
  288.3 0.8 copy.21
  (19 shorter events, 0.1 us)
Async XLA Ops:
  7.2 86.4 %all-gather.2.cloned.1.call-start = ((), (), s32[]{:S(2)}) async-start(), calls=%async_computation.4 | async-start | bytes 6389760 | tf_op jit(solution)/shard_map/all_gather | solution.py:26
  8.7 32.0 %copy-start.5 = (bf16[128,2048]{1,0:T(8,128)(2,1)S(1)}, bf16[128,2048]{1,0:T(8,128)(2,1)}, u32[]{:S(2)}) copy-start(bf16[128,2048]{1,0:T(8,128)(2,1)} %param.7) | copy-start | bytes 1572868
  40.7 59.5 %copy-start = (bf16[4,128,2048]{2,1,0:T(8,128)(2,1)}, bf16[4,128,2048]{2,1,0:T(8,128)(2,1)S(1)}, u32[]{:S(2)}) copy-start(bf16[4,128,2048]{2,1,0:T(8,128)(2,1)S(1)} %all_to_all.15) | copy-start | bytes 6291460
  42.4 30.0 %all-to-all-start = ((bf16[4,128,2048]{2,1,0:T(8,128)(2,1)}), bf16[4,128,2048]{2,1,0:T(8,128)(2,1)}, u32[]{:S(2)}, u32[]{:S(2)}) async-start(bf16[4,128,2048]{2,1,0:T(8,128)(2,1)} %broadcast_in_dim.6), calls=%async_computation | async-start | bytes 4194304 | tf_op jit(solution)/shard_map/all_to_all | solution.py:9
  46.9 239.2 %reduce-scatter.4.cloned.1.call-start = ((), (), s32[]{:S(2)}) async-start(), calls=%async_computation.5 | async-start | bytes 12779520
  93.6 6.6 %copy-start.8 = (bf16[2048,1536]{1,0:T(8,128)(2,1)S(1)}, bf16[2048,1536]{1,0:T(8,128)(2,1)}, u32[]{:S(2)}) copy-start(bf16[2048,1536]{1,0:T(8,128)(2,1)} %all-gather.2.cloned.1.call-done) | copy-start | bytes 18874372
  105.4 2.2 copy-start.1
  106.8 0.9 copy-start.3
  127.6 1.1 copy-start.4
  137.6 4.4 %copy-start.6 = (f32[32,768]{1,0:T(8,128)S(1)}, f32[32,768]{1,0:T(8,128)}, u32[]{:S(2)}) copy-start(f32[32,768]{1,0:T(8,128)} %param.13) | copy-start | bytes 294916
  137.6 5.3 %copy-start.7 = (f32[32,768]{1,0:T(8,128)S(1)}, f32[32,768]{1,0:T(8,128)}, u32[]{:S(2)}) copy-start(f32[32,768]{1,0:T(8,128)} %param.12) | copy-start | bytes 294916
  137.6 31.1 %all-to-all-start.2 = ((bf16[4,128,2048]{2,1,0:T(8,128)(2,1)}), bf16[4,128,2048]{2,1,0:T(8,128)(2,1)S(1)}, u32[]{:S(2)}, u32[]{:S(2)}) async-start(bf16[4,128,2048]{2,1,0:T(8,128)(2,1)} %bitcast.12), calls=%async_computation.2 | async-start | bytes 4194304 | tf_op jit(solution)/shard_map/all_to_all | solution.py:37
  144.3 143.0 %copy-start.2 = (f32[32,768]{0,1:T(8,128)S(1)}, f32[32,768]{0,1:T(8,128)}, u32[]{:S(2)}) copy-start(f32[32,768]{0,1:T(8,128)} %copy.19) | copy-start | bytes 294916
Sparse Core Ops, SparseCore 0:
  11.3 82.2 all-gather.1
  127.7 158.3 reduce-scatter.3
where the time goes:
time: 298 us; the launch traced here: 296 us
  waiting for transfers between devices  186 us (62%)
  blocking collectives  30.6 us (10%)
  matrix products  28 us (9%)
  local copies, waits for them, and re-layouts  24.2 us (8%)
  between operations  14.2 us (5%)
  starting transfers between devices  8.96 us (3%)
  other arithmetic  4.21 us (1%)
    unnamed x3, waiting for transfers between devices  116 us
    all_to_all x1, blocking collectives, from_everyone(): return lax.all_to_all(copies, axis, split_axis=0, concat_axis=0, tiled=True)  30.6 us
    all_to_all x1, waiting for transfers between devices, summed_on_arrival(): pieces = lax.all_to_all(in_blocks(x, dim, devices), axis, 0, 0, tiled=True)  24.5 us
    all_to_all x1, waiting for transfers between devices, from_everyone(): return lax.all_to_all(copies, axis, split_axis=0, concat_axis=0, tiled=True)  24.1 us
    all_gather x1, waiting for transfers between devices, sent_together(): result = lax.all_gather(both, axis, axis=dim, tiled=True)  21.1 us
    unnamed x27, local copies, waits for them, and re-layouts  20.2 us
    dot_general x1, matrix products, local(): lax.dot_general(rows_early, d_both, tokens_dim, preferred_element_type=jn...  7.33 us
    dot_general x1, matrix products, local(): gate_pre = jnp.dot(stacked, full_gate, preferred_element_type=jnp.float32)  6.56 us
  transfers between devices with their start and end apart: 4, of which 4 were waited for; matrix products, arithmetic and copies ran while one was open for 6% of the time, Pallas kernels for 0%

commit v1 on v0

v1 whole, which is shorter than its diff:
```python
import jax
import jax.numpy as jnp
from jax import lax
from jax.experimental import pallas as pl
from jax.experimental.pallas import tpu as pltpu
from jax.sharding import PartitionSpec as P

Z, X, C, Y = 8, 4, 2, 4
D, HID, ROWS, SHARD = 2048, 768, 128, 32
TOK = ROWS * Y
HALF = ROWS // 2
TILE = 256
TILES = HID // TILE
MESH = pl.DeviceIdType.MESH
F32, BF16 = jnp.float32, jnp.bfloat16
MAX_COPIES = 160
LOCAL_COPIES = 12


def sigmoid(v):
    return 0.5 * jnp.tanh(0.5 * v) + 0.5


def kernel(
    x_late, x_early, d_hidden, w_gate, w_up, gate_sum, up_sum,
    hidden_out, grad_out, gate_out, up_out,
    xe, xl, wg, wu, dh, sums, xt, xtp, dg, du, pdg, pdu, su, sg,
    up_stage, up_in, up_tot, up2_stage, up2_in,
    ga_stage, ga_in, ga_tot, ga2_stage, ga2_in,
    part, y_stage, y_in, grad, hid, send_sem, recv_sem, local_sem,
):
    fs = lax.axis_index("fs")
    y = lax.axis_index("tp")
    z, x, c = fs // (X * C), (fs // C) % X, fs % C

    def at(zz, xx, cc, yy):
        return {"fs": (zz * X + xx) * C + cc, "tp": yy}

    def zk(k):
        return lax.rem(z + (k + Z), Z)

    def xk(k):
        return lax.rem(x + (k + X), X)

    def yk(k):
        return lax.rem(y + (k + Y), Y)

    zp, zm = at(zk(1), x, c, y), at(zk(-1), x, c, y)
    xp, xm = at(z, xk(1), c, y), at(z, xk(-1), c, y)
    yp, ym = at(z, x, c, yk(1)), at(z, x, c, yk(-1))
    pal = at(z, x, 1 - c, y)

    local = []

    def load(src, dst):
        copy = pltpu.make_async_copy(src, dst, local_sem.at[len(local)])
        copy.start()
        local.append(copy)
        return copy

    in_xe = [load(x_early.at[pl.ds(h * HALF, HALF)], xe.at[y, h]) for h in range(2)]
    in_wu = load(w_up, wu.at[z, x, c])
    in_wg = load(w_gate, wg.at[z, x, c])
    in_xl = [load(x_late.at[pl.ds(h * HALF, HALF)], xl.at[y, h]) for h in range(2)]
    in_dh = load(d_hidden, dh)
    in_sums = [load(gate_sum, sums.at[0]), load(up_sum, sums.at[1])]

    barrier = pltpu.get_barrier_semaphore()
    for peer in (zp, zm, xp, xm, yp, ym, pal):
        pl.semaphore_signal(barrier, inc=1, device_id=peer, device_id_type=MESH)
    pl.semaphore_wait(barrier, 7)

    copies = []

    def send(src, dst, peer):
        i = len(copies)
        copy = pltpu.make_async_remote_copy(
            src_ref=src, dst_ref=dst, send_sem=send_sem.at[i], recv_sem=recv_sem.at[i],
            device_id=peer, device_id_type=MESH,
        )
        copy.start()
        copies.append(copy)
        return copy

    def pass_on(ref, peer):
        return send(ref, ref, peer)

    for copy in (in_wu, in_wg):
        copy.wait()
    uz_p, uz_m, ux, ux_relay = {}, {}, {}, {}

    def up_x(k):
        ref = wu.at[zk(k), x, c]
        ux[k] = (pass_on(ref, xp), pass_on(ref, xm))

    def up_x_relay(k):
        for copy in ux[k]:
            copy.wait_recv()
        zz = zk(k)
        ux_relay[k] = (
            pass_on(wu.at[zz, xk(-1), c, pl.ds(0, 16)], xp),
            pass_on(wu.at[zz, xk(1), c, pl.ds(16, 16)], xm),
        )

    pal_copies = []

    def up_row(k):
        for copy in ux_relay[k]:
            copy.wait_recv()
        pal_copies.append(pass_on(wu.at[zk(k), :, c], pal))

    uz_p[0] = pass_on(wu.at[z, x, c], zp)
    uz_m[0] = pass_on(wu.at[z, x, c], zm)
    gx = (pass_on(wg.at[z, x, c], xp), pass_on(wg.at[z, x, c], xm))
    up_x(0)
    for copy in in_xe:
        copy.wait()

    def y_own(ref):
        return {
            "l0": pass_on(ref.at[y, 0], yp),
            "r1": pass_on(ref.at[y, 1], ym),
            "l1": pass_on(ref.at[y, 1], yp),
            "r0": pass_on(ref.at[y, 0], ym),
        }

    def y_relay(ref, own):
        own["l0"].wait_recv()
        own["l2"] = pass_on(ref.at[yk(-1), 0], yp)
        own["r1"].wait_recv()
        own["r2"] = pass_on(ref.at[yk(1), 1], ym)

    def turn(block):
        columns = pl.ds(pl.multiple_of(block * ROWS, ROWS), ROWS)

        def step(zz, carry):
            rows = pl.ds(pl.multiple_of(zz * TILE, TILE), TILE)
            value = xe[block, :, :, rows].reshape(ROWS, TILE)
            xt[zz, :, :, :, columns] = value.T.reshape(X, C, SHARD, ROWS)
            return carry

        lax.fori_loop(0, Z, step, 0)

    early = y_own(xe)
    turn(y)

    for copy in gx:
        copy.wait_recv()
    gx_relay = (
        pass_on(wg.at[z, xk(-1), c, pl.ds(0, 16)], xp),
        pass_on(wg.at[z, xk(1), c, pl.ds(16, 16)], xm),
    )

    def up_z(k):
        uz_p[k - 1].wait_recv()
        uz_m[k - 1].wait_recv()
        left, right = wu.at[zk(-k), x, c], wu.at[zk(k), x, c]
        if k < 3:
            uz_p[k], uz_m[k] = pass_on(left, zp), pass_on(right, zm)
        elif k == 3:
            uz_p[k] = pass_on(left.at[pl.ds(0, 16)], zp)
            uz_m[k] = pass_on(right.at[pl.ds(16, 16)], zm)
        up_x(k)
        if k < 4:
            up_x(-k)

    gz_p, gz_m = {}, {}

    def gate_block(k, sub):
        return wg.at[zk(k), pl.ds(2 * sub, 2), c]

    def gate_z(k):
        if k == 0:
            for copy in gx_relay:
                copy.wait_recv()
        for sub in range(2):
            if k and (k < 4 or sub == 0):
                gz_p[k - 1, sub].wait_recv()
            if k < 3 or (k == 3 and sub == 0):
                gz_p[k, sub] = pass_on(gate_block(-k, sub), zp)
            if k and (k < 4 or sub == 1):
                gz_m[k - 1, sub].wait_recv()
            if k < 3 or (k == 3 and sub == 1):
                gz_m[k, sub] = pass_on(gate_block(k, sub), zm)
        pal_copies.append(pass_on(wg.at[zk(k), :, c], pal))
        if 0 < k < 4:
            pal_copies.append(pass_on(wg.at[zk(-k), :, c], pal))

    up_z(1)
    gate_z(0)
    up_x_relay(0)
    up_z(2)
    y_relay(xe, early)
    for copy in in_xl:
        copy.wait()
    late = y_own(xl)
    up_x_relay(1)
    up_x_relay(-1)
    gate_z(1)
    up_z(3)
    up_row(0)
    up_x_relay(2)
    up_x_relay(-2)
    up_z(4)
    gate_z(2)
    up_row(1)
    up_row(-1)
    up_x_relay(3)
    up_x_relay(-3)
    early["l1"].wait_recv()
    early["r0"].wait_recv()
    turn(yk(-1))
    turn(yk(1))
    up_x_relay(4)
    gate_z(3)
    up_row(2)
    up_row(-2)
    early["l2"].wait_recv()
    early["r2"].wait_recv()
    turn(yk(2))
    xt_copy = send(xt.at[:, :, 1 - c], xtp, pal)
    up_row(3)
    up_row(-3)
    up_row(4)
    gate_z(4)
    in_dh.wait()
    for copy in pal_copies:
        copy.wait_recv()

    def products(rows, tile):
        span = slice(tile * TILE, (tile + 1) * TILE)
        left = rows[...].reshape(TOK, D)
        gate = jnp.dot(left, wg[..., span].reshape(D, TILE), preferred_element_type=F32)
        up = jnp.dot(left, wu[..., span].reshape(D, TILE), preferred_element_type=F32)
        return gate, up, span

    pal_d = []
    for tile in range(TILES):
        gate, up, span = products(xe, tile)
        s = sigmoid(gate)
        cot = dh[:, span].astype(F32)
        du[:, span] = (cot * gate * s).astype(BF16)
        dg[:, span] = (cot * up * s * (1.0 + gate * (1.0 - s))).astype(BF16)
        pal_d.append((send(du.at[:, span], pdu.at[:, span], pal), send(dg.at[:, span], pdg.at[:, span], pal)))

    xt_copy.wait_recv()

    def weight_grad(which, own, other, total):
        for tile in range(TILES):
            span = slice(tile * TILE, (tile + 1) * TILE)
            pal_d[tile][which].wait_recv()
            mine = xt[:, :, c].reshape(Z * X * SHARD, TOK)
            theirs = xtp[...].reshape(Z * X * SHARD, TOK)
            value = jnp.dot(mine, own[:, span], preferred_element_type=F32)
            value = value + jnp.dot(theirs, other[:, span], preferred_element_type=F32)
            total[..., span] = value.reshape(Z, X, SHARD, TILE)

    weight_grad(0, du, pdu, su)

    def up_put(i, value, peer):
        up_stage[i] = value.astype(BF16)
        return send(up_stage.at[i], up_in.at[i], peer)

    u_a1 = up_put(0, su[pl.ds(0, 4), xk(2)], xp)
    u_b1 = up_put(1, su[pl.ds(4, 4), xk(2)], xm)
    u_a2 = up_put(2, su[pl.ds(4, 4), xk(1)], xp)
    u_b2 = up_put(3, su[pl.ds(0, 4), xk(-1)], xm)
    y_relay(xl, late)

    weight_grad(1, dg, pdg, sg)

    gs_p, gs_m = {}, {}

    def ga_index(right, k, sub):
        return (k * 2 + sub) * 2 + (0 if right else 1)

    def ga_send(k, sub):
        for right, sent, peer in ((True, gs_p, zp), (False, gs_m, zm)):
            half = sub if right else 1 - sub
            value = sg[zk(k if right else -k), pl.ds(2 * half, 2)]
            if (k + 1, sub) in sent:
                sent[k + 1, sub].wait_recv()
                value = value + ga_in[ga_index(right, k + 1, sub)].astype(F32)
            i = ga_index(right, k, sub)
            ga_stage[i] = value.astype(BF16)
            sent[k, sub] = send(ga_stage.at[i], ga_in.at[i], peer)

    ga_send(4, 0)
    ga_send(3, 1)

    contract = (((1,), (1,)), ((), ()))

    def input_grad(zz, carry):
        columns = pl.ds(pl.multiple_of(zz * TILE, TILE), TILE)
        value = lax.dot_general(dg[...], wg[zz].reshape(TILE, HID), contract, preferred_element_type=F32)
        value = value + lax.dot_general(du[...], wu[zz].reshape(TILE, HID), contract, preferred_element_type=F32)
        part[:, :, :, columns] = value.astype(BF16).reshape(Y, 2, HALF, TILE)
        return carry

    lax.fori_loop(0, Z, input_grad, 0)
    y_a1 = send(part.at[yk(2), 0], y_in.at[0], yp)
    y_b1 = send(part.at[yk(2), 1], y_in.at[1], ym)
    y_a2 = send(part.at[yk(1), 1], y_in.at[2], yp)
    y_b2 = send(part.at[yk(-1), 0], y_in.at[3], ym)

    u_a1.wait_recv()
    u_a3 = up_put(4, su[pl.ds(0, 4), xk(1)] + up_in[0].astype(F32), xp)
    u_b1.wait_recv()
    u_b3 = up_put(5, su[pl.ds(4, 4), xk(-1)] + up_in[1].astype(F32), xm)
    ga_send(3, 0)
    ga_send(2, 1)
    ga_send(2, 0)

    for key in ("l1", "r0", "l2", "r2"):
        late[key].wait_recv()

    hid_copies = []

    def late_tile(tile):
        gate, up, span = products(xl, tile)
        hid[:, span] = (gate * sigmoid(gate) * up).astype(BF16)
        hid_copies.append(load(hid.at[:, span], hidden_out.at[:, span]))

    late_tile(0)
    ga_send(1, 1)
    ga_send(1, 0)

    for copy in (u_a2, u_b2, u_a3, u_b3):
        copy.wait_recv()
    up_tot[pl.ds(0, 4)] = su[pl.ds(0, 4), x] + up_in[4].astype(F32) + up_in[3].astype(F32)
    up_tot[pl.ds(4, 4)] = su[pl.ds(4, 4), x] + up_in[2].astype(F32) + up_in[5].astype(F32)

    u2_p, u2_m = {}, {}

    def up2(k):
        for right, sent, peer in ((True, u2_p, zp), (False, u2_m, zm)):
            i = 2 * (k - 1) + (0 if right else 1)
            j = i + 2
            dest = zk(k if right else -k)
            h = 0 if right else 1
            near, far = pl.ds(16 * h, 16), pl.ds(16 * (1 - h), 16)
            if k == 4:
                up2_stage[i, near] = up_tot[dest, near].astype(BF16)
                sent[k] = send(up2_stage.at[i, near], up2_in.at[i, near], peer)
                continue
            sent[k + 1].wait_recv()
            if k == 3:
                up2_stage[i, near] = (up_tot[dest, near] + up2_in[j, near].astype(F32)).astype(BF16)
                up2_stage[i, far] = up_tot[dest, far].astype(BF16)
            else:
                up2_stage[i] = (up_tot[dest] + up2_in[j].astype(F32)).astype(BF16)
            sent[k] = send(up2_stage.at[i], up2_in.at[i], peer)

    up2(4)
    late_tile(1)
    up2(3)

    y_a1.wait_recv()
    y_stage[0] = (part[yk(1), 0].astype(F32) + y_in[0].astype(F32)).astype(BF16)
    y_a3 = send(y_stage.at[0], y_in.at[4], yp)
    y_b1.wait_recv()
    y_stage[1] = (part[yk(-1), 1].astype(F32) + y_in[1].astype(F32)).astype(BF16)
    y_b3 = send(y_stage.at[1], y_in.at[5], ym)

    up2(2)
    late_tile(2)
    up2(1)

    for sent in (gs_p, gs_m):
        sent[1, 0].wait_recv()
        sent[1, 1].wait_recv()
    for half in range(2):
        rows = pl.ds(2 * half, 2)
        ga_tot[rows] = (
            sg[z, rows]
            + ga_in[ga_index(True, 1, half)].astype(F32)
            + ga_in[ga_index(False, 1, 1 - half)].astype(F32)
        )

    lo, hi = pl.ds(0, 16), pl.ds(16, 16)
    ga2_stage[0, lo] = ga_tot[xk(2), lo].astype(BF16)
    g_a1 = send(ga2_stage.at[0, lo], ga2_in.at[0, lo], xp)
    ga2_stage[1, hi] = ga_tot[xk(2), hi].astype(BF16)
    g_b1 = send(ga2_stage.at[1, hi], ga2_in.at[1, hi], xm)
    g_a1.wait_recv()
    ga2_stage[2, lo] = (ga_tot[xk(1), lo] + ga2_in[0, lo].astype(F32)).astype(BF16)
    ga2_stage[2, hi] = ga_tot[xk(1), hi].astype(BF16)
    g_a3 = send(ga2_stage.at[2], ga2_in.at[2], xp)
    g_b1.wait_recv()
    ga2_stage[3, hi] = (ga_tot[xk(-1), hi] + ga2_in[1, hi].astype(F32)).astype(BF16)
    ga2_stage[3, lo] = ga_tot[xk(-1), lo].astype(BF16)
    g_b3 = send(ga2_stage.at[3], ga2_in.at[3], xm)

    for copy in in_sums:
        copy.wait()
    u2_p[1].wait_recv()
    u2_m[1].wait_recv()
    sums[1] = sums[1] + (up_tot[z] + up2_in[0].astype(F32) + up2_in[1].astype(F32))
    out_up = load(sums.at[1], up_out)

    g_a3.wait_recv()
    g_b3.wait_recv()
    sums[0] = sums[0] + (ga_tot[x] + ga2_in[2].astype(F32) + ga2_in[3].astype(F32))
    out_gate = load(sums.at[0], gate_out)

    for copy in (y_a2, y_b2, y_a3, y_b3):
        copy.wait_recv()
    grad[pl.ds(0, HALF)] = (part[y, 0].astype(F32) + y_in[4].astype(F32) + y_in[3].astype(F32)).astype(BF16)
    grad[pl.ds(HALF, HALF)] = (part[y, 1].astype(F32) + y_in[2].astype(F32) + y_in[5].astype(F32)).astype(BF16)
    out_grad = load(grad, grad_out)

    for copy in copies:
        copy.wait_send()
    for copy in (*hid_copies, out_up, out_gate, out_grad):
        copy.wait()


def local(*args):
    any_space = pl.BlockSpec(memory_space=pl.ANY)
    vmem = pltpu.VMEM
    flops = 4 * 2 * TOK * D * HID * 2
    return tuple(
        pl.pallas_call(
            kernel,
            out_shape=(
                jax.ShapeDtypeStruct((TOK, HID), BF16),
                jax.ShapeDtypeStruct((ROWS, D), BF16),
                jax.ShapeDtypeStruct((SHARD, HID), F32),
                jax.ShapeDtypeStruct((SHARD, HID), F32),
            ),
            in_specs=[any_space] * 7,
            out_specs=[any_space] * 4,
            scratch_shapes=[
                vmem((Y, 2, HALF, D), BF16),
                vmem((Y, 2, HALF, D), BF16),
                vmem((Z, X, C, SHARD, HID), BF16),
                vmem((Z, X, C, SHARD, HID), BF16),
                vmem((TOK, HID), BF16),
                vmem((2, SHARD, HID), F32),
                vmem((Z, X, C, SHARD, TOK), BF16),
                vmem((Z, X, SHARD, TOK), BF16),
                vmem((TOK, HID), BF16),
                vmem((TOK, HID), BF16),
                vmem((TOK, HID), BF16),
                vmem((TOK, HID), BF16),
                vmem((Z, X, SHARD, HID), F32),
                vmem((Z, X, SHARD, HID), F32),
                vmem((6, 4, SHARD, HID), BF16),
                vmem((6, 4, SHARD, HID), BF16),
                vmem((Z, SHARD, HID), F32),
                vmem((8, SHARD, HID), BF16),
                vmem((8, SHARD, HID), BF16),
                vmem((20, 2, SHARD, HID), BF16),
                vmem((20, 2, SHARD, HID), BF16),
                vmem((X, SHARD, HID), F32),
                vmem((4, SHARD, HID), BF16),
                vmem((4, SHARD, HID), BF16),
                vmem((Y, 2, HALF, D), BF16),
                vmem((2, HALF, D), BF16),
                vmem((6, HALF, D), BF16),
                vmem((ROWS, D), BF16),
                vmem((TOK, HID), BF16),
                pltpu.SemaphoreType.DMA((MAX_COPIES,)),
                pltpu.SemaphoreType.DMA((MAX_COPIES,)),
                pltpu.SemaphoreType.DMA((24,)),
            ],
            compiler_params=pltpu.CompilerParams(
                collective_id=0, has_side_effects=True, vmem_limit_bytes=63 * 1024 * 1024
            ),
            cost_estimate=pl.CostEstimate(flops=flops, bytes_accessed=8 << 20, transcendentals=0),
            name="layer",
        )(*args)
    )


def solution(mesh):
    return jax.shard_map(
        local,
        mesh=mesh,
        in_specs=(
            P(("fs", "tp"), None),
            P(("fs", "tp"), None),
            P("fs", "tp"),
            P("fs", "tp"),
            P("fs", "tp"),
            P("fs", "tp"),
            P("fs", "tp"),
        ),
        out_specs=(P("fs", "tp"), P(("fs", "tp"), None), P("fs", "tp"), P("fs", "tp")),
        check_vma=False,
    )
```

time: 298 us -> 90.3 us (0.30)
  waiting for transfers between devices: 186 us -> 0 us
  Pallas kernels: 0 us -> 84.8 us
  blocking collectives: 30.6 us -> 0 us
  matrix products: 28 us -> 0 us
  local copies, waits for them, and re-layouts: 24.2 us -> 4.66 us
  between operations: 14.2 us -> 0.65 us
  starting transfers between devices: 8.96 us -> 0 us
  other arithmetic: 4.21 us -> 0 us
    unnamed x3 -> x0, waiting for transfers between devices: 116 us -> none
    pallas_call x0 -> x1, Pallas kernels: none -> 84.8 us  [local(): pl.pallas_call(kernel, out_shape=(jax.ShapeDtypeStruct((TOK, HID), BF16),...]
    all_to_all x2 -> x0, waiting for transfers between devices: 48.6 us -> none  [the longest x1 24.5 us: summed_on_arrival(): pieces = lax.all_to_all(in_blocks(x, dim, devices), axis, 0, 0, tiled=True)]
    all_to_all x1 -> x0, blocking collectives: 30.6 us -> none  [from_everyone(): return lax.all_to_all(copies, axis, split_axis=0, concat_axis=0, tiled=True)]
    dot_general x5 -> x0, matrix products: 28 us -> none  [the longest x1 7.33 us: local(): lax.dot_general(rows_early, d_both, tokens_dim, preferred_element_type=jn...]
    all_gather x1 -> x0, waiting for transfers between devices: 21.1 us -> none  [sent_together(): result = lax.all_gather(both, axis, axis=dim, tiled=True)]
    unnamed x27 -> x10, local copies, waits for them, and re-layouts: 20.2 us -> 4.66 us
    all_to_all x2 -> x0, starting transfers between devices: 8.88 us -> none  [the longest x1 4.47 us: from_everyone(): return lax.all_to_all(copies, axis, split_axis=0, concat_axis=0, tiled=True)]
  transfers between devices with their start and end apart: 4 -> 0, of which waited for: 4 -> 0; matrix products, arithmetic and copies ran while one was open for 6% -> 0% of each run, Pallas kernels for 0% -> 0%
where the time goes in v1:
time: 90.3 us; the launch traced here: 90.1 us
  Pallas kernels  84.8 us (94%)
  local copies, waits for them, and re-layouts  4.66 us (5%)
    pallas_call x1, Pallas kernels, local(): pl.pallas_call(kernel, out_shape=(jax.ShapeDtypeStruct((TOK, HID), BF16),...  84.8 us
    unnamed x10, local copies, waits for them, and re-layouts  4.66 us

profile of v1, /device:TPU:2, one launch (start us, length us, event | category | flops | bytes accessed | tf_op | source)
XLA Modules:
  0.0 90.1 jit_solution(10376141890390585315)
XLA Ops:
  0.6 84.8 %layer.1 = (bf16[512,768]{1,0:T(8,128)(2,1)}, bf16[128,2048]{1,0:T(8,128)(2,1)}, f32[32,768]{1,0:T(8,128)}, f32[32,768]{1,0:T(8,128)}) custom-call(bf16[128,2048]{1,0:T(8,128)(2,1)} %x_late.1, bf16[128,2048]{1,0:T(8,128)(2,1)} %x_early.1, bf16[512,768]{1,0:T(8,128)(2,1)} %d_hidden.1, bf16[32,768]{1,0:T(8,128)(2,1)} %w_gate.1, bf16[32,768]{1,0:T(8,128)(2,1)} %w_up.1, ...), custom_call_target="tpu_custom_call" | custom-call | flops 12884901888 | bytes 8388608 | tf_op jit(solution)/shard_map/layer/pallas_call | solution.py:423
  85.4 0.0 copy-start
  85.4 2.1 %copy.15 = bf16[512,768]{1,0:T(8,128)(2,1)} copy(bf16[512,768]{1,0:T(8,128)(2,1)} %get-tuple-element.8) | data formatting | bytes 1572864
  87.6 0.0 copy-done
  87.6 0.0 copy-start.2
  87.6 0.8 copy.16
  88.4 0.2 copy-done.2
  88.5 0.0 copy-start.1
  88.5 0.6 copy.17
  89.2 0.3 copy-done.1
  89.5 0.6 copy.18
Async XLA Ops:
  85.4 2.1 %copy-start = (bf16[128,2048]{1,0:T(8,128)(2,1)S(1)}, bf16[128,2048]{1,0:T(8,128)(2,1)}, u32[]{:S(2)}) copy-start(bf16[128,2048]{1,0:T(8,128)(2,1)} %get-tuple-element.9) | copy-start | bytes 1572868
  87.6 1.0 %copy-start.2 = (f32[32,768]{1,0:T(8,128)S(1)}, f32[32,768]{1,0:T(8,128)}, u32[]{:S(2)}) copy-start(f32[32,768]{1,0:T(8,128)} %get-tuple-element.10) | copy-start | bytes 294916
  88.5 0.9 %copy-start.1 = (f32[32,768]{1,0:T(8,128)S(1)}, f32[32,768]{1,0:T(8,128)}, u32[]{:S(2)}) copy-start(f32[32,768]{1,0:T(8,128)} %get-tuple-element.11) | copy-start | bytes 294916

commit v2 on v0

v2 whole, which is shorter than its diff:
```python
import jax
import jax.numpy as jnp
from jax import lax
from jax.experimental import pallas as pl
from jax.experimental.pallas import tpu as pltpu
from jax.sharding import PartitionSpec as P

Z, X, C, Y = 8, 4, 2, 4
D, HID, ROWS, SHARD = 2048, 768, 128, 32
BOTH = 2 * HID
NA = 640
NB = BOTH - NA
TOK = ROWS * Y
HALF = ROWS // 2
TILE = 256
MESH = pl.DeviceIdType.MESH
F32, BF16 = jnp.float32, jnp.bfloat16
DIRS = (1, -1)
COPIES, SENDS = 202, 100
ORDER = (
    ("own",), ("t", 0), ("ax1",), ("bz", 1), ("az", 0, 1), ("bx", 0), ("ax2",), ("ar", 0), ("az", 1, 1),
    ("az", -1, 1), ("xer",), ("xlo",), ("bx", 1), ("bz", 2), ("br", 0), ("az", 0, 2), ("az", 2, 1), ("ar", 1),
    ("az", 1, 2), ("br", 1), ("az", -1, 2), ("bz", 3), ("t", 1), ("az", 0, 3), ("bx", 2), ("f", 0), ("f", 1),
    ("az", 2, 2), ("ar", 2), ("az", 1, 3), ("az", -1, 3), ("bz", 4), ("az", 0, 4), ("bx", 3), ("br", 2),
    ("t", 2), ("az", 2, 3), ("ar", 3), ("az", 1, 4), ("az", -1, 4), ("bx", 4), ("f", 2), ("br", 3),
    ("az", 2, 4), ("ar", 4), ("br", 4), ("f", 3), ("f", 4), ("f2",), ("e", 1), ("e", 0), ("xlr",), ("e", 2),
    ("i", 3), ("i", 1), ("i", 0), ("w", 4), ("w", 3), ("y1", 0), ("i", 2), ("y1", 1), ("sz", 2, 3), ("sx", 4),
    ("sz", 1, 3), ("w", 2), ("sz", -1, 3), ("l", 1), ("sz", 2, 2), ("sx", 3), ("st", 4), ("sz", 0, 3),
    ("y2", 0), ("w", 1), ("sz", 1, 2), ("sx", 2), ("sz", -1, 2), ("w", 0), ("sz", 2, 1), ("l", 0), ("st", 3),
    ("sb", 3), ("sz", 0, 2), ("l", 2), ("sx", 1), ("sz", -1, 1), ("y2", 1), ("sz", 1, 1), ("at", 2),
    ("st", 2), ("sb", 2), ("sx", 0), ("sz", 0, 1), ("at", -1), ("at", 1), ("yf", 0), ("st", 1), ("sa",),
    ("sb", 1), ("at", 0), ("st", 0), ("yf", 1), ("fa",), ("fb",),
)


def sigmoid(v):
    return 0.5 * jnp.tanh(0.5 * v) + 0.5


def rows_of(k):
    return (k,) if k in (0, 4) else (k, -k)


def kernel(
    x_late, x_early, d_hidden, w_gate, w_up, gate_sum, up_sum,
    hidden_out, grad_out, gate_out, up_out,
    xe, xl, w, dh, sums, xt, xtp, d, pd, acc, s, ta, tb,
    a_stage, a_in, b_stage, b_in, part, y_stage, y_in,
    send_sem, recv_sem, local_sem,
):
    fs = lax.axis_index("fs")
    y = lax.axis_index("tp")
    z, x, c = fs // (X * C), (fs // C) % X, fs % C

    def zk(k):
        return lax.rem(z + (k + Z), Z)

    def xk(k):
        return lax.rem(x + (k + X), X)

    def yk(k):
        return lax.rem(y + (k + Y), Y)

    def at(zz, xx, cc, yy):
        return {"fs": (zz * X + xx) * C + cc, "tp": yy}

    zp = {k: at(zk(k), x, c, y) for k in DIRS}
    xp = {k: at(z, xk(k), c, y) for k in DIRS}
    yp = {k: at(z, x, c, yk(k)) for k in DIRS}
    pal = at(z, x, 1 - c, y)

    local = []

    def load(src, dst):
        copy = pltpu.make_async_copy(src, dst, local_sem.at[len(local)])
        copy.start()
        local.append(copy)
        return copy

    in_w = [
        load(w_up, w.at[z, x, c, :, pl.ds(HID, HID)]),
        load(w_gate, w.at[z, x, c, :, pl.ds(0, HID)]),
    ]
    in_xe = [load(x_early.at[pl.ds(h * HALF, HALF)], xe.at[y, h]) for h in range(2)]
    in_xl = [load(x_late.at[pl.ds(h * HALF, HALF)], xl.at[y, h]) for h in range(2)]
    in_dh = load(d_hidden, dh)
    in_sums = [load(gate_sum, sums.at[:, pl.ds(0, HID)]), load(up_sum, sums.at[:, pl.ds(HID, HID)])]

    with jax.named_scope("entry"):
        barrier = pltpu.get_barrier_semaphore()
        for peer in (*zp.values(), *xp.values(), *yp.values(), pal):
            pl.semaphore_signal(barrier, inc=1, device_id=peer, device_id_type=MESH)
        pl.semaphore_wait(barrier, 7)

    msgs, order = {}, []

    def send(key, src, dst, peer):
        i = len(msgs)
        if i >= SENDS:
            order[i - SENDS].wait_send()
        copy = pltpu.make_async_remote_copy(
            src_ref=src, dst_ref=dst, send_sem=send_sem.at[i % SENDS], recv_sem=recv_sem.at[i],
            device_id=peer, device_id_type=MESH,
        )
        order.append(copy)
        copy.start()
        msgs[key] = copy

    def push(key, ref, peer):
        send(key, ref, ref, peer)

    def wait(*key):
        msgs[key].wait_recv()

    def half(k):
        return pl.ds(0, 16) if k > 0 else pl.ds(16, 16)

    ALL = pl.ds(0, SHARD)
    CA, CB = pl.ds(0, NA), pl.ds(NA, NB)

    def own():
        for copy in in_w:
            copy.wait()
        for k in DIRS:
            push(("bz", 0, k), w.at[z, x, c, :, CB], zp[k])
        for k in DIRS:
            push(("ax", k), w.at[z, x, c, :, CA], xp[k])
        for k in DIRS:
            push(("bx", 0, k), w.at[z, x, c, :, CB], xp[k])
        for k in DIRS:
            push(("az", 0, 0, k), w.at[z, x, c, :, CA], zp[k])
        for copy in in_xe:
            copy.wait()
        y_own("xe", xe)

    def y_own(name, ref):
        for i in range(2):
            for k in DIRS:
                h = i if k > 0 else 1 - i
                push((name, i, k), ref.at[y, h], yp[k])

    def y_relay(name, ref):
        for k in DIRS:
            wait(name, 0, k)
            push((name, 2, k), ref.at[yk(-k), 0 if k > 0 else 1], yp[k])

    def xl_own():
        for copy in in_xl:
            copy.wait()
        y_own("xl", xl)

    def turn(block):
        tokens = pl.ds(pl.multiple_of(block * ROWS, ROWS), ROWS)

        def step(zz, carry):
            span = pl.ds(pl.multiple_of(zz * TILE, TILE), TILE)
            value = xe[block, :, :, span].reshape(ROWS, TILE)
            xt[zz, :, :, :, tokens] = value.T.reshape(X, C, SHARD, ROWS)
            return carry

        lax.fori_loop(0, Z, step, 0)
        return tokens

    def turns(which):
        if which == 1:
            for k in DIRS:
                wait("xe", 1, k)
        if which == 2:
            for k in DIRS:
                wait("xe", 2, k)
        for k in (1, -1) if which == 1 else (which,):
            tokens = turn(yk(k))
            send(("xt", k), xt.at[:, :, 1 - c, :, tokens], xtp.at[:, :, :, tokens], pal)

    def ax1():
        for k in DIRS:
            wait("ax", k)
        for k in DIRS:
            push(("axr", k), w.at[z, xk(-k), c, half(k), CA], xp[k])
        for j in DIRS:
            for k in DIRS:
                push(("az", j, 0, k), w.at[z, xk(j), c, :, CA], zp[k])

    def ax2():
        for k in DIRS:
            wait("axr", k)
        for k in DIRS:
            push(("az", 2, 0, k), w.at[z, xk(2), c, :, CA], zp[k])

    def az(j, n):
        for k in DIRS:
            wait("az", j, n - 1, k)
        if n < 4:
            for k in DIRS:
                rows = half(k) if n == 3 else ALL
                push(("az", j, n, k), w.at[zk(-k * n), xk(j), c, rows, CA], zp[k])

    def ar(n):
        for r in rows_of(n):
            push(("ar", r), w.at[zk(r), :, c, :, CA], pal)

    def bz(n):
        for k in DIRS:
            wait("bz", n - 1, k)
        if n < 4:
            for k in DIRS:
                rows = half(k) if n == 3 else ALL
                push(("bz", n, k), w.at[zk(-k * n), x, c, rows, CB], zp[k])
        for r in rows_of(n):
            for k in DIRS:
                push(("bx", r, k), w.at[zk(r), x, c, :, CB], xp[k])

    def bx(n):
        for r in rows_of(n):
            for k in DIRS:
                wait("bx", r, k)
                push(("bxr", r, k), w.at[zk(r), xk(-k), c, half(k), CB], xp[k])

    def br(n):
        for r in rows_of(n):
            for k in DIRS:
                wait("bxr", r, k)
            push(("br", r), w.at[zk(r), :, c, :, CB], pal)

    def dot(a, b):
        return jnp.dot(a, b, preferred_element_type=F32)

    near = (0, 1, -1)

    def f(n):
        left, right = [], []
        for r in rows_of(n):
            wait("ar", r)
            wait("br", r)
            span = pl.ds(pl.multiple_of(zk(r) * TILE, TILE), TILE)
            left.append(jnp.concatenate([xe[yk(k), :, :, span].reshape(ROWS, TILE) for k in near], axis=0))
            right.append(w[zk(r)].reshape(TILE, BOTH))
        value = dot(jnp.concatenate(left, axis=1), jnp.concatenate(right, axis=0))
        for i, k in enumerate(near):
            piece = value[i * ROWS : (i + 1) * ROWS]
            acc[yk(k)] = piece if n == 0 else acc[yk(k)] + piece

    def f2():
        for copy in (in_dh, *in_sums):
            copy.wait()
        left = xe[yk(2)].reshape(ROWS, D)
        for t in range(BOTH // TILE):
            span = pl.ds(t * TILE, TILE)
            acc[yk(2), :, span] = dot(left, w[..., span].reshape(D, TILE))

    def e(t):
        lo, hi = pl.ds(t * TILE, TILE), pl.ds(HID + t * TILE, TILE)
        gate = acc[..., lo].reshape(TOK, TILE)
        up = acc[..., hi].reshape(TOK, TILE)
        sig = sigmoid(gate)
        cot = dh[:, lo].astype(F32) * sig
        d[:, lo] = (cot * up * (1.0 + gate * (1.0 - sig))).astype(BF16)
        d[:, hi] = (cot * gate).astype(BF16)
        send(("d", t, 0), d.at[:, lo], pd.at[:, lo], pal)
        send(("d", t, 1), d.at[:, hi], pd.at[:, hi], pal)

    lates = []

    def late(t):
        if not lates:
            for i in (1, 2):
                for k in DIRS:
                    wait("xl", i, k)
        lates.append(t)
        lo, hi = pl.ds(t * TILE, TILE), pl.ds(HID + t * TILE, TILE)
        left = xl[...].reshape(TOK, D)
        gate = dot(left, w[..., lo].reshape(D, TILE))
        up = dot(left, w[..., hi].reshape(D, TILE))
        hidden_out[:, lo] = (gate * sigmoid(gate) * up).astype(BF16)

    slots = {}

    def slot(kind, key):
        return slots.setdefault((kind, key), sum(1 for name in slots if name[0] == kind))

    def sent(kind, key, value, peer, rows=ALL, more=None, more_rows=None):
        stage, into = (a_stage, a_in) if kind == "a" else (b_stage, b_in)
        i = slot(kind, key)
        stage[i, rows] = value.astype(BF16)
        if more is not None:
            stage[i, more_rows] = more.astype(BF16)
            rows = ALL
        send(key, stage.at[i, rows], into.at[i, rows], peer)

    def came(kind, *key):
        wait(*key)
        ref = a_in if kind == "a" else b_in
        return ref, slot(kind, key)

    def wgrad(n):
        if n == 4:
            for t in range(3):
                wait("d", t, 0)
                wait("d", t, 1)
            for k in (0, 1, -1, 2):
                wait("xt", k)
        rows = rows_of(n)
        mine = jnp.concatenate([xt[zk(r), :, c].reshape(X * SHARD, TOK) for r in rows], axis=0)
        theirs = jnp.concatenate([xtp[zk(r)].reshape(X * SHARD, TOK) for r in rows], axis=0)
        value = dot(mine, d[...]) + dot(theirs, pd[...])
        for i, r in enumerate(rows):
            s[zk(r)] = value[i * X * SHARD : (i + 1) * X * SHARD].reshape(X, SHARD, BOTH)
        for r in rows:
            for k in DIRS:
                sent("b", ("sx", r, 2, k), s[zk(r), xk(2), half(k), CB], xp[k], half(k))
        if n == 4:
            for j in (2, 1, -1, 0):
                for k in DIRS:
                    sent("a", ("sz", j, 4, k), s[zk(4), xk(j), half(k), CA], zp[k], half(k))

    def onward(kind, before, key, own, peer, partly, k):
        ref, i = came(kind, *before)
        if partly:
            mine, rest = half(k), half(-k)
            sent(kind, key, own(mine) + ref[i, mine].astype(F32), peer, mine, own(rest), rest)
        else:
            sent(kind, key, own(ALL) + ref[i].astype(F32), peer)

    def sx(n):
        for r in rows_of(n):
            for k in DIRS:
                onward("b", ("sx", r, 2, k), ("sx", r, 1, k), lambda q: s[zk(r), xk(k), q, CB], xp[k], True, k)

    def both(kind, own, *key):
        value = own
        for k in DIRS:
            ref, i = came(kind, *key, k)
            value = value + ref[i].astype(F32)
        return value

    def st(n):
        for r in rows_of(n):
            tb[zk(r)] = both("b", s[zk(r), x, :, CB], "sx", r, 1)
        if n == 4:
            for k in DIRS:
                sent("b", ("sb", 4, k), tb[zk(4), half(k)], zp[k], half(k))

    def sb(n):
        for k in DIRS:
            onward("b", ("sb", n + 1, k), ("sb", n, k), lambda q: tb[zk(k * n), q], zp[k], n == 3, k)

    def fb():
        value = sums[:, CB] + both("b", tb[z], "sb", 1)
        gate_out[:, pl.ds(NA, HID - NA)] = value[:, : HID - NA]
        up_out[...] = value[:, HID - NA :]

    def sz(j, n):
        for k in DIRS:
            onward("a", ("sz", j, n + 1, k), ("sz", j, n, k), lambda q: s[zk(k * n), xk(j), q, CA], zp[k], n == 3, k)

    def at_x(j):
        ta[xk(j)] = both("a", s[z, xk(j), :, CA], "sz", j, 1)
        if j == 2:
            for k in DIRS:
                sent("a", ("sa", 2, k), ta[xk(2), half(k)], xp[k], half(k))

    def sa():
        for k in DIRS:
            onward("a", ("sa", 2, k), ("sa", 1, k), lambda q: ta[xk(k), q], xp[k], True, k)

    def fa():
        gate_out[:, CA] = sums[:, CA] + both("a", ta[x], "sa", 1)

    def igrad(n):
        span = pl.ds(n * 2 * TILE, 2 * TILE)
        weights = w[2 * n : 2 * n + 2].reshape(2 * TILE, BOTH)
        value = lax.dot_general(d[...], weights, (((1,), (1,)), ((), ())), preferred_element_type=F32)
        part[..., span] = value.astype(BF16).reshape(Y, 2, HALF, 2 * TILE)

    def y_cols(h):
        return pl.ds(h * (D // 2), D // 2)

    def y1(h):
        for m, which in ((2, 2), (3, 1)):
            for k in DIRS:
                side = (0 if k > 0 else 1) if m == 2 else (1 if k > 0 else 0)
                i = 4 * h + 2 * (m - 2) + (0 if k > 0 else 1)
                send(("y", h, m, k), part.at[yk(which * k), side, :, y_cols(h)], y_in.at[i], yp[k])

    def y2(h):
        for k in DIRS:
            i = 0 if k > 0 else 1
            wait("y", h, 2, k)
            value = part[yk(k), i, :, y_cols(h)].astype(F32) + y_in[4 * h + i].astype(F32)
            y_stage[2 * h + i] = value.astype(BF16)
            send(("y", h, 1, k), y_stage.at[2 * h + i], y_in.at[8 + 2 * h + i], yp[k])

    def yf(h):
        for k in DIRS:
            wait("y", h, 1, k)
            wait("y", h, 3, k)
        for side in range(2):
            value = part[y, side, :, y_cols(h)].astype(F32)
            value = value + y_in[8 + 2 * h + side].astype(F32)
            value = value + y_in[4 * h + 2 + (1 - side)].astype(F32)
            grad_out[pl.ds(side * HALF, HALF), y_cols(h)] = value.astype(BF16)

    tasks = {
        "own": own, "t": turns, "xer": lambda: y_relay("xe", xe), "xlo": xl_own,
        "xlr": lambda: y_relay("xl", xl), "ax1": ax1, "ax2": ax2, "az": az, "ar": ar, "bz": bz, "bx": bx,
        "br": br, "f": f, "f2": f2, "e": e, "w": wgrad, "sx": sx, "st": st, "sb": sb, "fb": fb, "sz": sz,
        "at": at_x, "sa": sa, "fa": fa, "i": igrad, "y1": y1, "y2": y2, "yf": yf, "l": late,
    }
    for name, *args in ORDER:
        with jax.named_scope("_".join(map(str, (name, *args)))):
            tasks[name](*args)
    with jax.named_scope("drain"):
        for copy in order[-SENDS:]:
            copy.wait_send()


def local(*args):
    hbm_space = pl.BlockSpec(memory_space=pltpu.HBM)
    vmem_space = pl.BlockSpec(memory_space=pltpu.VMEM)
    vmem = pltpu.VMEM
    return tuple(
        pl.pallas_call(
            kernel,
            out_shape=OUTS,
            in_specs=[hbm_space] * 7,
            out_specs=[vmem_space] * 4,
            scratch_shapes=[
                vmem((Y, 2, HALF, D), BF16),
                vmem((Y, 2, HALF, D), BF16),
                vmem((Z, X, C, SHARD, BOTH), BF16),
                vmem((TOK, HID), BF16),
                vmem((SHARD, BOTH), F32),
                vmem((Z, X, C, SHARD, TOK), BF16),
                vmem((Z, X, SHARD, TOK), BF16),
                vmem((TOK, BOTH), BF16),
                vmem((TOK, BOTH), BF16),
                vmem((Y, ROWS, BOTH), F32),
                vmem((Z, X, SHARD, BOTH), F32),
                vmem((X, SHARD, NA), F32),
                vmem((Z, SHARD, NB), F32),
                vmem((36, SHARD, NA), BF16),
                vmem((36, SHARD, NA), BF16),
                vmem((40, SHARD, NB), BF16),
                vmem((40, SHARD, NB), BF16),
                vmem((Y, 2, HALF, D), BF16),
                vmem((4, HALF, D // 2), BF16),
                vmem((12, HALF, D // 2), BF16),
                pltpu.SemaphoreType.DMA((SENDS,)),
                pltpu.SemaphoreType.DMA((COPIES,)),
                pltpu.SemaphoreType.DMA((16,)),
            ],
            compiler_params=pltpu.CompilerParams(
                collective_id=0, has_side_effects=True, vmem_limit_bytes=VMEM_MIB * 1024 * 1024
            ),
            cost_estimate=pl.CostEstimate(flops=8 * TOK * D * BOTH, bytes_accessed=8 << 20, transcendentals=0),
            name="layer",
        )(*args)
    )


OUTS = (
    jax.ShapeDtypeStruct((TOK, HID), BF16),
    jax.ShapeDtypeStruct((ROWS, D), BF16),
    jax.ShapeDtypeStruct((SHARD, HID), F32),
    jax.ShapeDtypeStruct((SHARD, HID), F32),
)
VMEM_MIB = 60


def solution(mesh):
    return jax.shard_map(
        local,
        mesh=mesh,
        in_specs=(
            P(("fs", "tp"), None),
            P(("fs", "tp"), None),
            P("fs", "tp"),
            P("fs", "tp"),
            P("fs", "tp"),
            P("fs", "tp"),
            P("fs", "tp"),
        ),
        out_specs=(P("fs", "tp"), P(("fs", "tp"), None), P("fs", "tp"), P("fs", "tp")),
        check_vma=False,
    )
```

time: 298 us -> 72.8 us (0.24)
  waiting for transfers between devices: 186 us -> 0 us
  Pallas kernels: 0 us -> 67.1 us
  blocking collectives: 30.6 us -> 0 us
  matrix products: 28 us -> 0 us
  local copies, waits for them, and re-layouts: 24.2 us -> 4.66 us
  between operations: 14.2 us -> 0.65 us
  starting transfers between devices: 8.96 us -> 0 us
  other arithmetic: 4.21 us -> 0 us
    unnamed x3 -> x0, waiting for transfers between devices: 116 us -> none
    pallas_call x0 -> x1, Pallas kernels: none -> 67.1 us  [local(): pl.pallas_call(kernel, out_shape=OUTS, in_specs=[hbm_space] * 7, out_spec...]
    all_to_all x2 -> x0, waiting for transfers between devices: 48.6 us -> none  [the longest x1 24.5 us: summed_on_arrival(): pieces = lax.all_to_all(in_blocks(x, dim, devices), axis, 0, 0, tiled=True)]
    all_to_all x1 -> x0, blocking collectives: 30.6 us -> none  [from_everyone(): return lax.all_to_all(copies, axis, split_axis=0, concat_axis=0, tiled=True)]
    dot_general x5 -> x0, matrix products: 28 us -> none  [the longest x1 7.33 us: local(): lax.dot_general(rows_early, d_both, tokens_dim, preferred_element_type=jn...]
    all_gather x1 -> x0, waiting for transfers between devices: 21.1 us -> none  [sent_together(): result = lax.all_gather(both, axis, axis=dim, tiled=True)]
    unnamed x27 -> x10, local copies, waits for them, and re-layouts: 20.2 us -> 4.66 us
    all_to_all x2 -> x0, starting transfers between devices: 8.88 us -> none  [the longest x1 4.47 us: from_everyone(): return lax.all_to_all(copies, axis, split_axis=0, concat_axis=0, tiled=True)]
  transfers between devices with their start and end apart: 4 -> 0, of which waited for: 4 -> 0; matrix products, arithmetic and copies ran while one was open for 6% -> 0% of each run, Pallas kernels for 0% -> 0%
where the time goes in v2:
time: 72.8 us; the launch traced here: 72.4 us
  Pallas kernels  67.1 us (92%)
  local copies, waits for them, and re-layouts  4.66 us (6%)
    pallas_call x1, Pallas kernels, local(): pl.pallas_call(kernel, out_shape=OUTS, in_specs=[hbm_space] * 7, out_spec...  67.1 us
    unnamed x10, local copies, waits for them, and re-layouts  4.66 us

profile of v2, /device:TPU:2, one launch (start us, length us, event | category | flops | bytes accessed | tf_op | source)
XLA Modules:
  0.0 72.4 jit_solution(654651904099072198)
XLA Ops:
  0.6 67.1 %layer.1 = (bf16[512,768]{1,0:T(8,128)(2,1)}, bf16[128,2048]{1,0:T(8,128)(2,1)}, f32[32,768]{1,0:T(8,128)}, f32[32,768]{1,0:T(8,128)}) custom-call(bf16[128,2048]{1,0:T(8,128)(2,1)} %x_late.1, bf16[128,2048]{1,0:T(8,128)(2,1)} %x_early.1, bf16[512,768]{1,0:T(8,128)(2,1)} %d_hidden.1, bf16[32,768]{1,0:T(8,128)(2,1)} %w_gate.1, bf16[32,768]{1,0:T(8,128)(2,1)} %w_up.1, ...), custom_call_target="tpu_custom_call" | custom-call | flops 12884901888 | bytes 8388608 | tf_op jit(solution)/shard_map/layer/pallas_call | solution.py:422
  67.7 0.0 copy-start
  67.7 2.1 %copy.15 = bf16[512,768]{1,0:T(8,128)(2,1)} copy(bf16[512,768]{1,0:T(8,128)(2,1)} %get-tuple-element.8) | data formatting | bytes 1572864
  69.9 0.0 copy-done
  69.9 0.0 copy-start.2
  69.9 0.8 %copy.16 = bf16[128,2048]{1,0:T(8,128)(2,1)} copy(bf16[128,2048]{1,0:T(8,128)(2,1)S(1)} %copy-done) | data formatting | bytes 1048576
  70.7 0.2 copy-done.2
  70.8 0.0 copy-start.1
  70.8 0.6 copy.17
  71.5 0.3 copy-done.1
  71.8 0.6 copy.18
Async XLA Ops:
  67.7 2.1 %copy-start = (bf16[128,2048]{1,0:T(8,128)(2,1)S(1)}, bf16[128,2048]{1,0:T(8,128)(2,1)}, u32[]{:S(2)}) copy-start(bf16[128,2048]{1,0:T(8,128)(2,1)} %get-tuple-element.9) | copy-start | bytes 1572868
  69.9 1.0 %copy-start.2 = (f32[32,768]{1,0:T(8,128)S(1)}, f32[32,768]{1,0:T(8,128)}, u32[]{:S(2)}) copy-start(f32[32,768]{1,0:T(8,128)} %get-tuple-element.10) | copy-start | bytes 294916
  70.8 0.9 %copy-start.1 = (f32[32,768]{1,0:T(8,128)S(1)}, f32[32,768]{1,0:T(8,128)}, u32[]{:S(2)}) copy-start(f32[32,768]{1,0:T(8,128)} %get-tuple-element.11) | copy-start | bytes 294916

commit v3 on v2

--- a/solution.py
+++ b/solution.py
@@ -16,7 +16,7 @@
 MESH = pl.DeviceIdType.MESH
 F32, BF16 = jnp.float32, jnp.bfloat16
 DIRS = (1, -1)
-COPIES, SENDS = 202, 100
+GROUPS, SIZED = 96, 11264
 ORDER = (
     ("own",), ("t", 0), ("ax1",), ("bz", 1), ("az", 0, 1), ("bx", 0), ("ax2",), ("ar", 0), ("az", 1, 1),
     ("az", -1, 1), ("xer",), ("xlo",), ("bx", 1), ("bz", 2), ("br", 0), ("az", 0, 2), ("az", 2, 1), ("ar", 1),
@@ -41,11 +41,30 @@
     return (k,) if k in (0, 4) else (k, -k)
 
 
+def group_of(key):
+    name = key[0]
+    if name in ("xt", "d"):
+        return (name,)
+    if name == "xe":
+        return (name, key[1])
+    if name == "xl":
+        return (name, min(key[1], 1))
+    if name in ("ar", "br"):
+        return ("row", abs(key[1]))
+    if name in ("bx", "bxr"):
+        return (name, abs(key[1]))
+    if name == "sx":
+        return (name, abs(key[1]), key[2])
+    if name == "y":
+        return (name, key[1], 2 if key[2] == 2 else 1)
+    return key[:-1]
+
+
 def kernel(
     x_late, x_early, d_hidden, w_gate, w_up, gate_sum, up_sum,
     hidden_out, grad_out, gate_out, up_out,
     xe, xl, w, dh, sums, xt, xtp, d, pd, acc, s, ta, tb,
-    a_stage, a_in, b_stage, b_in, part, y_stage, y_in,
+    a_stage, a_in, b_stage, b_in, part, y_stage, y_in, hid, grad, sized,
     send_sem, recv_sem, local_sem,
 ):
     fs = lax.axis_index("fs")
@@ -76,6 +95,11 @@
         copy.start()
         local.append(copy)
         return copy
+
+    stores = []
+
+    def store(src, dst):
+        stores.append(load(src, dst))
 
     in_w = [
         load(w_up, w.at[z, x, c, :, pl.ds(HID, HID)]),
@@ -92,25 +116,36 @@
             pl.semaphore_signal(barrier, inc=1, device_id=peer, device_id_type=MESH)
         pl.semaphore_wait(barrier, 7)
 
-    msgs, order = {}, []
+    groups, links = {}, {}
+
+    def taken(sem, size):
+        ref = sized.at[pl.ds(0, size // 512)]
+        pltpu.make_async_copy(ref, ref, sem).wait()
 
     def send(key, src, dst, peer):
-        i = len(msgs)
-        if i >= SENDS:
-            order[i - SENDS].wait_send()
-        copy = pltpu.make_async_remote_copy(
-            src_ref=src, dst_ref=dst, send_sem=send_sem.at[i % SENDS], recv_sem=recv_sem.at[i],
+        group, link = group_of(key), id(peer)
+        into = groups.setdefault(group, [len(groups), 0, False])
+        out = links.setdefault(link, [len(links), 0])
+        if into[2]:
+            raise ValueError(key)
+        pltpu.make_async_remote_copy(
+            src_ref=src, dst_ref=dst, send_sem=send_sem.at[out[0]], recv_sem=recv_sem.at[into[0]],
             device_id=peer, device_id_type=MESH,
-        )
-        order.append(copy)
-        copy.start()
-        msgs[key] = copy
+        ).start()
+        size = src.dtype.itemsize
+        for extent in src.shape:
+            size *= extent
+        into[1] += size
+        out[1] += size
 
     def push(key, ref, peer):
         send(key, ref, ref, peer)
 
-    def wait(*key):
-        msgs[key].wait_recv()
+    def wait(*group):
+        into = groups[group]
+        if not into[2]:
+            into[2] = True
+            taken(recv_sem.at[into[0]], into[1])
 
     def half(k):
         return pl.ds(0, 16) if k > 0 else pl.ds(16, 16)
@@ -140,8 +175,8 @@
                 push((name, i, k), ref.at[y, h], yp[k])
 
     def y_relay(name, ref):
-        for k in DIRS:
-            wait(name, 0, k)
+        wait(name, 0)
+        for k in DIRS:
             push((name, 2, k), ref.at[yk(-k), 0 if k > 0 else 1], yp[k])
 
     def xl_own():
@@ -163,18 +198,15 @@
 
     def turns(which):
         if which == 1:
-            for k in DIRS:
-                wait("xe", 1, k)
+            wait("xe", 1)
         if which == 2:
-            for k in DIRS:
-                wait("xe", 2, k)
+            wait("xe", 2)
         for k in (1, -1) if which == 1 else (which,):
             tokens = turn(yk(k))
             send(("xt", k), xt.at[:, :, 1 - c, :, tokens], xtp.at[:, :, :, tokens], pal)
 
     def ax1():
-        for k in DIRS:
-            wait("ax", k)
+        wait("ax")
         for k in DIRS:
             push(("axr", k), w.at[z, xk(-k), c, half(k), CA], xp[k])
         for j in DIRS:
@@ -182,14 +214,12 @@
                 push(("az", j, 0, k), w.at[z, xk(j), c, :, CA], zp[k])
 
     def ax2():
-        for k in DIRS:
-            wait("axr", k)
+        wait("axr")
         for k in DIRS:
             push(("az", 2, 0, k), w.at[z, xk(2), c, :, CA], zp[k])
 
     def az(j, n):
-        for k in DIRS:
-            wait("az", j, n - 1, k)
+        wait("az", j, n - 1)
         if n < 4:
             for k in DIRS:
                 rows = half(k) if n == 3 else ALL
@@ -200,8 +230,7 @@
             push(("ar", r), w.at[zk(r), :, c, :, CA], pal)
 
     def bz(n):
-        for k in DIRS:
-            wait("bz", n - 1, k)
+        wait("bz", n - 1)
         if n < 4:
             for k in DIRS:
                 rows = half(k) if n == 3 else ALL
@@ -211,15 +240,14 @@
                 push(("bx", r, k), w.at[zk(r), x, c, :, CB], xp[k])
 
     def bx(n):
-        for r in rows_of(n):
-            for k in DIRS:
-                wait("bx", r, k)
+        wait("bx", n)
+        for r in rows_of(n):
+            for k in DIRS:
                 push(("bxr", r, k), w.at[zk(r), xk(-k), c, half(k), CB], xp[k])
 
     def br(n):
-        for r in rows_of(n):
-            for k in DIRS:
-                wait("bxr", r, k)
+        wait("bxr", n)
+        for r in rows_of(n):
             push(("br", r), w.at[zk(r), :, c, :, CB], pal)
 
     def dot(a, b):
@@ -229,9 +257,8 @@
 
     def f(n):
         left, right = [], []
-        for r in rows_of(n):
-            wait("ar", r)
-            wait("br", r)
+        wait("row", n)
+        for r in rows_of(n):
             span = pl.ds(pl.multiple_of(zk(r) * TILE, TILE), TILE)
             left.append(jnp.concatenate([xe[yk(k), :, :, span].reshape(ROWS, TILE) for k in near], axis=0))
             right.append(w[zk(r)].reshape(TILE, BOTH))
@@ -263,15 +290,14 @@
 
     def late(t):
         if not lates:
-            for i in (1, 2):
-                for k in DIRS:
-                    wait("xl", i, k)
+            wait("xl", 1)
         lates.append(t)
         lo, hi = pl.ds(t * TILE, TILE), pl.ds(HID + t * TILE, TILE)
         left = xl[...].reshape(TOK, D)
         gate = dot(left, w[..., lo].reshape(D, TILE))
         up = dot(left, w[..., hi].reshape(D, TILE))
-        hidden_out[:, lo] = (gate * sigmoid(gate) * up).astype(BF16)
+        hid[:, lo] = (gate * sigmoid(gate) * up).astype(BF16)
+        store(hid.at[:, lo], hidden_out.at[:, lo])
 
     slots = {}
 
@@ -288,17 +314,14 @@
         send(key, stage.at[i, rows], into.at[i, rows], peer)
 
     def came(kind, *key):
-        wait(*key)
+        wait(*group_of(key))
         ref = a_in if kind == "a" else b_in
         return ref, slot(kind, key)
 
     def wgrad(n):
         if n == 4:
-            for t in range(3):
-                wait("d", t, 0)
-                wait("d", t, 1)
-            for k in (0, 1, -1, 2):
-                wait("xt", k)
+            wait("d")
+            wait("xt")
         rows = rows_of(n)
         mine = jnp.concatenate([xt[zk(r), :, c].reshape(X * SHARD, TOK) for r in rows], axis=0)
         theirs = jnp.concatenate([xtp[zk(r)].reshape(X * SHARD, TOK) for r in rows], axis=0)
@@ -345,9 +368,9 @@
             onward("b", ("sb", n + 1, k), ("sb", n, k), lambda q: tb[zk(k * n), q], zp[k], n == 3, k)
 
     def fb():
-        value = sums[:, CB] + both("b", tb[z], "sb", 1)
-        gate_out[:, pl.ds(NA, HID - NA)] = value[:, : HID - NA]
-        up_out[...] = value[:, HID - NA :]
+        sums[:, CB] = sums[:, CB] + both("b", tb[z], "sb", 1)
+        store(sums.at[:, pl.ds(NA, HID - NA)], gate_out.at[:, pl.ds(NA, HID - NA)])
+        store(sums.at[:, pl.ds(HID, HID)], up_out)
 
     def sz(j, n):
         for k in DIRS:
@@ -364,7 +387,8 @@
             onward("a", ("sa", 2, k), ("sa", 1, k), lambda q: ta[xk(k), q], xp[k], True, k)
 
     def fa():
-        gate_out[:, CA] = sums[:, CA] + both("a", ta[x], "sa", 1)
+        sums[:, CA] = sums[:, CA] + both("a", ta[x], "sa", 1)
+        store(sums.at[:, CA], gate_out.at[:, CA])
 
     def igrad(n):
         span = pl.ds(n * 2 * TILE, 2 * TILE)
@@ -385,20 +409,19 @@
     def y2(h):
         for k in DIRS:
             i = 0 if k > 0 else 1
-            wait("y", h, 2, k)
+            wait("y", h, 2)
             value = part[yk(k), i, :, y_cols(h)].astype(F32) + y_in[4 * h + i].astype(F32)
             y_stage[2 * h + i] = value.astype(BF16)
             send(("y", h, 1, k), y_stage.at[2 * h + i], y_in.at[8 + 2 * h + i], yp[k])
 
     def yf(h):
-        for k in DIRS:
-            wait("y", h, 1, k)
-            wait("y", h, 3, k)
+        wait("y", h, 1)
         for side in range(2):
             value = part[y, side, :, y_cols(h)].astype(F32)
             value = value + y_in[8 + 2 * h + side].astype(F32)
             value = value + y_in[4 * h + 2 + (1 - side)].astype(F32)
-            grad_out[pl.ds(side * HALF, HALF), y_cols(h)] = value.astype(BF16)
+            grad[pl.ds(side * HALF, HALF), y_cols(h)] = value.astype(BF16)
+        store(grad.at[:, y_cols(h)], grad_out.at[:, y_cols(h)])
 
     tasks = {
         "own": own, "t": turns, "xer": lambda: y_relay("xe", xe), "xlo": xl_own,
@@ -410,20 +433,33 @@
         with jax.named_scope("_".join(map(str, (name, *args)))):
             tasks[name](*args)
     with jax.named_scope("drain"):
-        for copy in order[-SENDS:]:
-            copy.wait_send()
+        for i, size in links.values():
+            taken(send_sem.at[i], size)
+        for copy in stores:
+            copy.wait()
+
+
+def finish(*refs):
+    ins, outs, held, sems = refs[:4], refs[4:8], refs[8:12], refs[12]
+    into = [pltpu.make_async_copy(a, b, sems.at[0, i]) for i, (a, b) in enumerate(zip(ins, held))]
+    out = [pltpu.make_async_copy(a, b, sems.at[1, i]) for i, (a, b) in enumerate(zip(held, outs))]
+    for copy in into:
+        copy.start()
+    for first, second in zip(into, out):
+        first.wait()
+        second.start()
+    for copy in out:
+        copy.wait()
 
 
 def local(*args):
-    hbm_space = pl.BlockSpec(memory_space=pltpu.HBM)
-    vmem_space = pl.BlockSpec(memory_space=pltpu.VMEM)
+    any_space = pl.BlockSpec(memory_space=pl.ANY)
     vmem = pltpu.VMEM
-    return tuple(
-        pl.pallas_call(
+    held = pl.pallas_call(
             kernel,
             out_shape=OUTS,
-            in_specs=[hbm_space] * 7,
-            out_specs=[vmem_space] * 4,
+            in_specs=[any_space] * 7,
+            out_specs=[any_space] * 4,
             scratch_shapes=[
                 vmem((Y, 2, HALF, D), BF16),
                 vmem((Y, 2, HALF, D), BF16),
@@ -445,9 +481,12 @@
                 vmem((Y, 2, HALF, D), BF16),
                 vmem((4, HALF, D // 2), BF16),
                 vmem((12, HALF, D // 2), BF16),
-                pltpu.SemaphoreType.DMA((SENDS,)),
-                pltpu.SemaphoreType.DMA((COPIES,)),
-                pltpu.SemaphoreType.DMA((16,)),
+                vmem((TOK, HID), BF16),
+                vmem((ROWS, D), BF16),
+                vmem((SIZED, 128), F32),
+                pltpu.SemaphoreType.DMA((7,)),
+                pltpu.SemaphoreType.DMA((GROUPS,)),
+                pltpu.SemaphoreType.DMA((20,)),
             ],
             compiler_params=pltpu.CompilerParams(
                 collective_id=0, has_side_effects=True, vmem_limit_bytes=VMEM_MIB * 1024 * 1024
@@ -455,6 +494,15 @@
             cost_estimate=pl.CostEstimate(flops=8 * TOK * D * BOTH, bytes_accessed=8 << 20, transcendentals=0),
             name="layer",
         )(*args)
+    return tuple(
+        pl.pallas_call(
+            finish,
+            out_shape=OUTS,
+            in_specs=[any_space] * 4,
+            out_specs=[any_space] * 4,
+            scratch_shapes=[*(vmem(a.shape, a.dtype) for a in OUTS), pltpu.SemaphoreType.DMA((2, 4))],
+            name="finish",
+        )(*held)
     )
 
 

time: 72.8 us -> 69 us (0.948)
  local copies, waits for them, and re-layouts: 4.66 us -> 0 us
    unnamed x10 -> x0, local copies, waits for them, and re-layouts: 4.66 us -> none
    pallas_call x1 -> x2, Pallas kernels: 67.1 us -> 67.7 us  [the longest x1 65.4 us: local(): pl.pallas_call(kernel, out_shape=OUTS, in_specs=[any_space] * 7, out_spec...]
where the time goes in v3:
time: 69 us; the launch traced here: 68.4 us
  Pallas kernels  67.7 us (98%)
    pallas_call x1, Pallas kernels, local(): pl.pallas_call(kernel, out_shape=OUTS, in_specs=[any_space] * 7, out_spec...  65.4 us
    pallas_call x1, Pallas kernels, local(): pl.pallas_call(finish, out_shape=OUTS, in_specs=[any_space] * 4, out_spec...  2.31 us

profile of v3, /device:TPU:2, one launch (start us, length us, event | category | flops | bytes accessed | tf_op | source)
XLA Modules:
  0.0 68.4 jit_solution(17208518289118099248)
XLA Ops:
  0.6 65.4 %layer.1 = (bf16[512,768]{1,0:T(8,128)(2,1)}, bf16[128,2048]{1,0:T(8,128)(2,1)}, f32[32,768]{1,0:T(8,128)}, f32[32,768]{1,0:T(8,128)}) custom-call(bf16[128,2048]{1,0:T(8,128)(2,1)} %x_late.1, bf16[128,2048]{1,0:T(8,128)(2,1)} %x_early.1, bf16[512,768]{1,0:T(8,128)(2,1)} %d_hidden.1, bf16[32,768]{1,0:T(8,128)(2,1)} %w_gate.1, bf16[32,768]{1,0:T(8,128)(2,1)} %w_up.1, ...), custom_call_target="tpu_custom_call" | custom-call | flops 12884901888 | bytes 8388608 | tf_op jit(solution)/shard_map/layer/pallas_call | solution.py:458
  66.1 2.3 %finish.1 = (bf16[512,768]{1,0:T(8,128)(2,1)}, bf16[128,2048]{1,0:T(8,128)(2,1)}, f32[32,768]{1,0:T(8,128)}, f32[32,768]{1,0:T(8,128)}) custom-call(bf16[512,768]{1,0:T(8,128)(2,1)} %get-tuple-element.8.refs_0_, bf16[128,2048]{1,0:T(8,128)(2,1)} %get-tuple-element.9.refs_1_, f32[32,768]{1,0:T(8,128)} %get-tuple-element.10.refs_2_, ...), custom_call_target="tpu_custom_call" | custom-call | tf_op jit(solution)/shard_map/finish/pallas_call | solution.py:498

commit v4 on v3

--- a/solution.py
+++ b/solution.py
@@ -18,18 +18,19 @@
 DIRS = (1, -1)
 GROUPS, SIZED = 96, 11264
 ORDER = (
-    ("own",), ("t", 0), ("ax1",), ("bz", 1), ("az", 0, 1), ("bx", 0), ("ax2",), ("ar", 0), ("az", 1, 1),
-    ("az", -1, 1), ("xer",), ("xlo",), ("bx", 1), ("bz", 2), ("br", 0), ("az", 0, 2), ("az", 2, 1), ("ar", 1),
-    ("az", 1, 2), ("br", 1), ("az", -1, 2), ("bz", 3), ("t", 1), ("az", 0, 3), ("bx", 2), ("f", 0), ("f", 1),
-    ("az", 2, 2), ("ar", 2), ("az", 1, 3), ("az", -1, 3), ("bz", 4), ("az", 0, 4), ("bx", 3), ("br", 2),
-    ("t", 2), ("az", 2, 3), ("ar", 3), ("az", 1, 4), ("az", -1, 4), ("bx", 4), ("f", 2), ("br", 3),
-    ("az", 2, 4), ("ar", 4), ("br", 4), ("f", 3), ("f", 4), ("f2",), ("e", 1), ("e", 0), ("xlr",), ("e", 2),
-    ("i", 3), ("i", 1), ("i", 0), ("w", 4), ("w", 3), ("y1", 0), ("i", 2), ("y1", 1), ("sz", 2, 3), ("sx", 4),
-    ("sz", 1, 3), ("w", 2), ("sz", -1, 3), ("l", 1), ("sz", 2, 2), ("sx", 3), ("st", 4), ("sz", 0, 3),
-    ("y2", 0), ("w", 1), ("sz", 1, 2), ("sx", 2), ("sz", -1, 2), ("w", 0), ("sz", 2, 1), ("l", 0), ("st", 3),
-    ("sb", 3), ("sz", 0, 2), ("l", 2), ("sx", 1), ("sz", -1, 1), ("y2", 1), ("sz", 1, 1), ("at", 2),
-    ("st", 2), ("sb", 2), ("sx", 0), ("sz", 0, 1), ("at", -1), ("at", 1), ("yf", 0), ("st", 1), ("sa",),
-    ("sb", 1), ("at", 0), ("st", 0), ("yf", 1), ("fa",), ("fb",),
+    ("own",), ("ax1",), ("bz", 1), ("az0",), ("bx", 0), ("bzx", 1), ("ax2",), ("bz", 2), ("az", 0, 1),
+    ("bzx", 2), ("az", -1, 1), ("t", 0), ("az", 1, 1), ("xer",), ("ar", 0), ("bx", 1), ("bz", 3),
+    ("az", 2, 1), ("xlo",), ("br", 0), ("bzx", 3), ("bx", 2), ("ar", 1), ("az", 0, 2), ("az", -1, 2),
+    ("az", 1, 2), ("bzx", 4), ("br", 1), ("az", 2, 2), ("t", 1), ("ar", 2), ("bx", 3), ("az", 0, 3),
+    ("az", -1, 3), ("f", 0), ("az", 1, 3), ("br", 2), ("f", 1), ("az", 2, 3), ("bx", 4), ("ar", 3), ("t", 2),
+    ("az", -1, 4), ("br", 3), ("f", 2), ("f2",), ("az", 1, 4), ("az", 0, 4), ("az", 2, 4), ("ar", 4),
+    ("br", 4), ("f", 3), ("f", 4), ("e", -1), ("xlr",), ("e", 2), ("e", 0), ("e", 1), ("i", 3), ("i", 2),
+    ("i", 0), ("w", 4), ("w", 3), ("w", 2), ("sz", 2, 3), ("sx", 4), ("y1", 1), ("sz", 1, 3), ("i", 1),
+    ("sz", -1, 3), ("y1", 0), ("sz", 0, 3), ("sx", 3), ("sz", 2, 2), ("w", 1), ("st", 4), ("w", 0),
+    ("sz", 1, 2), ("sz", -1, 2), ("sx", 2), ("sz", 2, 1), ("st", 3), ("sb", 3), ("sz", 0, 2), ("y2", 1),
+    ("bz", 4), ("sx", 1), ("sz", 1, 1), ("l", 2), ("sz", -1, 1), ("y2", 0), ("st", 2), ("at", 2), ("sb", 2),
+    ("l", 1), ("sx", 0), ("l", 0), ("at", 1), ("st", 1), ("sz", 0, 1), ("sb", 1), ("at", -1), ("sa",),
+    ("at", 0), ("yf", 1), ("st", 0), ("fa",), ("fb",), ("yf", 0),
 )
 
 
@@ -107,7 +108,7 @@
     ]
     in_xe = [load(x_early.at[pl.ds(h * HALF, HALF)], xe.at[y, h]) for h in range(2)]
     in_xl = [load(x_late.at[pl.ds(h * HALF, HALF)], xl.at[y, h]) for h in range(2)]
-    in_dh = load(d_hidden, dh)
+    in_dh = [load(d_hidden.at[pl.ds(i * ROWS, ROWS)], dh.at[i]) for i in range(Y)]
     in_sums = [load(gate_sum, sums.at[:, pl.ds(0, HID)]), load(up_sum, sums.at[:, pl.ds(HID, HID)])]
 
     with jax.named_scope("entry"):
@@ -209,6 +210,9 @@
         wait("ax")
         for k in DIRS:
             push(("axr", k), w.at[z, xk(-k), c, half(k), CA], xp[k])
+
+    def az0():
+        wait("ax")
         for j in DIRS:
             for k in DIRS:
                 push(("az", j, 0, k), w.at[z, xk(j), c, :, CA], zp[k])
@@ -235,6 +239,9 @@
             for k in DIRS:
                 rows = half(k) if n == 3 else ALL
                 push(("bz", n, k), w.at[zk(-k * n), x, c, rows, CB], zp[k])
+
+    def bzx(n):
+        wait("bz", n - 1)
         for r in rows_of(n):
             for k in DIRS:
                 push(("bx", r, k), w.at[zk(r), x, c, :, CB], xp[k])
@@ -253,38 +260,33 @@
     def dot(a, b):
         return jnp.dot(a, b, preferred_element_type=F32)
 
-    near = (0, 1, -1)
+    def rows_product(rows, blocks):
+        spans = [pl.ds(pl.multiple_of(zk(r) * TILE, TILE), TILE) for r in rows]
+        left = [[xe[yk(b), :, :, q].reshape(ROWS, TILE) for q in spans] for b in blocks]
+        left = jnp.concatenate([jnp.concatenate(q, axis=1) for q in left], axis=0)
+        right = jnp.concatenate([w[zk(r)].reshape(TILE, BOTH) for r in rows], axis=0)
+        value = dot(left, right)
+        return [(yk(b), value[i * ROWS : (i + 1) * ROWS]) for i, b in enumerate(blocks)]
 
     def f(n):
-        left, right = [], []
         wait("row", n)
-        for r in rows_of(n):
-            span = pl.ds(pl.multiple_of(zk(r) * TILE, TILE), TILE)
-            left.append(jnp.concatenate([xe[yk(k), :, :, span].reshape(ROWS, TILE) for k in near], axis=0))
-            right.append(w[zk(r)].reshape(TILE, BOTH))
-        value = dot(jnp.concatenate(left, axis=1), jnp.concatenate(right, axis=0))
-        for i, k in enumerate(near):
-            piece = value[i * ROWS : (i + 1) * ROWS]
-            acc[yk(k)] = piece if n == 0 else acc[yk(k)] + piece
+        for block, piece in rows_product(rows_of(n), (0, 1, -1) if n < 3 else (0, 1, -1, 2)):
+            acc[block] = piece if n == 0 else acc[block] + piece
 
     def f2():
-        for copy in (in_dh, *in_sums):
+        for copy in (*in_dh, *in_sums):
             copy.wait()
-        left = xe[yk(2)].reshape(ROWS, D)
-        for t in range(BOTH // TILE):
-            span = pl.ds(t * TILE, TILE)
-            acc[yk(2), :, span] = dot(left, w[..., span].reshape(D, TILE))
-
-    def e(t):
-        lo, hi = pl.ds(t * TILE, TILE), pl.ds(HID + t * TILE, TILE)
-        gate = acc[..., lo].reshape(TOK, TILE)
-        up = acc[..., hi].reshape(TOK, TILE)
+        for block, piece in rows_product((0, 1, -1, 2, -2), (2,)):
+            acc[block] = piece
+
+    def e(b):
+        block = yk(b)
+        gate, up = acc[block, :, :HID], acc[block, :, HID:]
         sig = sigmoid(gate)
-        cot = dh[:, lo].astype(F32) * sig
-        d[:, lo] = (cot * up * (1.0 + gate * (1.0 - sig))).astype(BF16)
-        d[:, hi] = (cot * gate).astype(BF16)
-        send(("d", t, 0), d.at[:, lo], pd.at[:, lo], pal)
-        send(("d", t, 1), d.at[:, hi], pd.at[:, hi], pal)
+        cot = dh[block].astype(F32) * sig
+        d[block, :, :HID] = (cot * up * (1.0 + gate * (1.0 - sig))).astype(BF16)
+        d[block, :, HID:] = (cot * gate).astype(BF16)
+        send(("d", b), d.at[block], pd.at[block], pal)
 
     lates = []
 
@@ -325,7 +327,7 @@
         rows = rows_of(n)
         mine = jnp.concatenate([xt[zk(r), :, c].reshape(X * SHARD, TOK) for r in rows], axis=0)
         theirs = jnp.concatenate([xtp[zk(r)].reshape(X * SHARD, TOK) for r in rows], axis=0)
-        value = dot(mine, d[...]) + dot(theirs, pd[...])
+        value = dot(mine, d[...].reshape(TOK, BOTH)) + dot(theirs, pd[...].reshape(TOK, BOTH))
         for i, r in enumerate(rows):
             s[zk(r)] = value[i * X * SHARD : (i + 1) * X * SHARD].reshape(X, SHARD, BOTH)
         for r in rows:
@@ -393,7 +395,7 @@
     def igrad(n):
         span = pl.ds(n * 2 * TILE, 2 * TILE)
         weights = w[2 * n : 2 * n + 2].reshape(2 * TILE, BOTH)
-        value = lax.dot_general(d[...], weights, (((1,), (1,)), ((), ())), preferred_element_type=F32)
+        value = lax.dot_general(d[...].reshape(TOK, BOTH), weights, (((1,), (1,)), ((), ())), preferred_element_type=F32)
         part[..., span] = value.astype(BF16).reshape(Y, 2, HALF, 2 * TILE)
 
     def y_cols(h):
@@ -425,7 +427,7 @@
 
     tasks = {
         "own": own, "t": turns, "xer": lambda: y_relay("xe", xe), "xlo": xl_own,
-        "xlr": lambda: y_relay("xl", xl), "ax1": ax1, "ax2": ax2, "az": az, "ar": ar, "bz": bz, "bx": bx,
+        "xlr": lambda: y_relay("xl", xl), "ax1": ax1, "az0": az0, "bzx": bzx, "ax2": ax2, "az": az, "ar": ar, "bz": bz, "bx": bx,
         "br": br, "f": f, "f2": f2, "e": e, "w": wgrad, "sx": sx, "st": st, "sb": sb, "fb": fb, "sz": sz,
         "at": at_x, "sa": sa, "fa": fa, "i": igrad, "y1": y1, "y2": y2, "yf": yf, "l": late,
     }
@@ -464,12 +466,12 @@
                 vmem((Y, 2, HALF, D), BF16),
                 vmem((Y, 2, HALF, D), BF16),
                 vmem((Z, X, C, SHARD, BOTH), BF16),
-                vmem((TOK, HID), BF16),
+                vmem((Y, ROWS, HID), BF16),
                 vmem((SHARD, BOTH), F32),
                 vmem((Z, X, C, SHARD, TOK), BF16),
                 vmem((Z, X, SHARD, TOK), BF16),
-                vmem((TOK, BOTH), BF16),
-                vmem((TOK, BOTH), BF16),
+                vmem((Y, ROWS, BOTH), BF16),
+                vmem((Y, ROWS, BOTH), BF16),
                 vmem((Y, ROWS, BOTH), F32),
                 vmem((Z, X, SHARD, BOTH), F32),
                 vmem((X, SHARD, NA), F32),

time: 69 us -> 66.3 us (0.961)
  Pallas kernels: 67.7 us -> 65.5 us
    pallas_call x1, Pallas kernels: 65.4 us -> 63.2 us  [local(): pl.pallas_call(kernel, out_shape=OUTS, in_specs=[any_space] * 7, out_spec...]
where the time goes in v4:
time: 66.3 us; the launch traced here: 66.2 us
  Pallas kernels  65.5 us (99%)
    pallas_call x1, Pallas kernels, local(): pl.pallas_call(kernel, out_shape=OUTS, in_specs=[any_space] * 7, out_spec...  63.2 us
    pallas_call x1, Pallas kernels, local(): pl.pallas_call(finish, out_shape=OUTS, in_specs=[any_space] * 4, out_spec...  2.31 us

profile of v4, /device:TPU:2, one launch (start us, length us, event | category | flops | bytes accessed | tf_op | source)
XLA Modules:
  0.0 66.2 jit_solution(5381841330575936014)
XLA Ops:
  0.6 63.2 %layer.1 = (bf16[512,768]{1,0:T(8,128)(2,1)}, bf16[128,2048]{1,0:T(8,128)(2,1)}, f32[32,768]{1,0:T(8,128)}, f32[32,768]{1,0:T(8,128)}) custom-call(bf16[128,2048]{1,0:T(8,128)(2,1)} %x_late.1, bf16[128,2048]{1,0:T(8,128)(2,1)} %x_early.1, bf16[512,768]{1,0:T(8,128)(2,1)} %d_hidden.1, bf16[32,768]{1,0:T(8,128)(2,1)} %w_gate.1, bf16[32,768]{1,0:T(8,128)(2,1)} %w_up.1, ...), custom_call_target="tpu_custom_call" | custom-call | flops 12884901888 | bytes 8388608 | tf_op jit(solution)/shard_map/layer/pallas_call | solution.py:460
  63.8 2.3 %finish.1 = (bf16[512,768]{1,0:T(8,128)(2,1)}, bf16[128,2048]{1,0:T(8,128)(2,1)}, f32[32,768]{1,0:T(8,128)}, f32[32,768]{1,0:T(8,128)}) custom-call(bf16[512,768]{1,0:T(8,128)(2,1)} %get-tuple-element.8.refs_0_, bf16[128,2048]{1,0:T(8,128)(2,1)} %get-tuple-element.9.refs_1_, f32[32,768]{1,0:T(8,128)} %get-tuple-element.10.refs_2_, ...), custom_call_target="tpu_custom_call" | custom-call | tf_op jit(solution)/shard_map/finish/pallas_call | solution.py:500

commit v5 on v4

--- a/solution.py
+++ b/solution.py
@@ -16,21 +16,21 @@
 MESH = pl.DeviceIdType.MESH
 F32, BF16 = jnp.float32, jnp.bfloat16
 DIRS = (1, -1)
-GROUPS, SIZED = 96, 11264
+GROUPS, SIZED = 79, 11264
 ORDER = (
-    ("own",), ("ax1",), ("bz", 1), ("az0",), ("bx", 0), ("bzx", 1), ("ax2",), ("bz", 2), ("az", 0, 1),
-    ("bzx", 2), ("az", -1, 1), ("t", 0), ("az", 1, 1), ("xer",), ("ar", 0), ("bx", 1), ("bz", 3),
-    ("az", 2, 1), ("xlo",), ("br", 0), ("bzx", 3), ("bx", 2), ("ar", 1), ("az", 0, 2), ("az", -1, 2),
-    ("az", 1, 2), ("bzx", 4), ("br", 1), ("az", 2, 2), ("t", 1), ("ar", 2), ("bx", 3), ("az", 0, 3),
-    ("az", -1, 3), ("f", 0), ("az", 1, 3), ("br", 2), ("f", 1), ("az", 2, 3), ("bx", 4), ("ar", 3), ("t", 2),
-    ("az", -1, 4), ("br", 3), ("f", 2), ("f2",), ("az", 1, 4), ("az", 0, 4), ("az", 2, 4), ("ar", 4),
-    ("br", 4), ("f", 3), ("f", 4), ("e", -1), ("xlr",), ("e", 2), ("e", 0), ("e", 1), ("i", 3), ("i", 2),
-    ("i", 0), ("w", 4), ("w", 3), ("w", 2), ("sz", 2, 3), ("sx", 4), ("y1", 1), ("sz", 1, 3), ("i", 1),
-    ("sz", -1, 3), ("y1", 0), ("sz", 0, 3), ("sx", 3), ("sz", 2, 2), ("w", 1), ("st", 4), ("w", 0),
-    ("sz", 1, 2), ("sz", -1, 2), ("sx", 2), ("sz", 2, 1), ("st", 3), ("sb", 3), ("sz", 0, 2), ("y2", 1),
-    ("bz", 4), ("sx", 1), ("sz", 1, 1), ("l", 2), ("sz", -1, 1), ("y2", 0), ("st", 2), ("at", 2), ("sb", 2),
-    ("l", 1), ("sx", 0), ("l", 0), ("at", 1), ("st", 1), ("sz", 0, 1), ("sb", 1), ("at", -1), ("sa",),
-    ("at", 0), ("yf", 1), ("st", 0), ("fa",), ("fb",), ("yf", 0),
+    ("own",), ("bz", 1, 1), ("ax1",), ("bz", 1, -1), ("bx", 0), ("bzx", 1), ("az0",), ("t", 0), ("az", 0, 1),
+    ("bz", 2, 1), ("ax2",), ("bzx", 2), ("bz", 2, -1), ("bx", 1), ("br", 0), ("ar", 0), ("xer",),
+    ("az", 1, 1), ("az", -1, 1), ("bz", 3, 1), ("az", 2, 1), ("ar", 1), ("bx", 2), ("bzx", 3), ("az", 0, 2),
+    ("az", 1, 2), ("xlo",), ("az", -1, 2), ("t", 1), ("bzx", 4), ("az", 2, 2), ("br", 1), ("az", 0, 3),
+    ("ar", 2), ("bx", 3), ("f", 0), ("az", 1, 3), ("br", 2), ("az", -1, 3), ("f", 1), ("bx", 4), ("az", 2, 3),
+    ("t", 2), ("f", 2), ("ar", 3), ("br", 3), ("f2",), ("br", 4), ("az", 1, 4), ("az", -1, 4), ("az", 0, 4),
+    ("az", 2, 4), ("ar", 4), ("f", 3), ("f", 4), ("e", 2), ("e", 0), ("e", 1), ("xlr",), ("e", -1), ("i", 3),
+    ("i", 2), ("y1", 1), ("w", 4), ("w", 3), ("sz", 2, 3), ("sx", 4), ("w", 2), ("sz", 1, 3), ("sz", -1, 3),
+    ("sx", 3), ("sz", 0, 3), ("i", 1), ("st", 4), ("sz", 2, 2), ("w", 1), ("sz", 1, 2), ("i", 0),
+    ("sz", -1, 2), ("y1", 0), ("sx", 2), ("sz", 0, 2), ("y2", 1), ("st", 3), ("sb", 3), ("sz", 2, 1),
+    ("l", 1), ("w", 0), ("sz", -1, 1), ("sz", 1, 1), ("l", 2), ("sx", 1), ("st", 2), ("sb", 2), ("at", 2),
+    ("sz", 0, 1), ("y2", 0), ("at", 1), ("sx", 0), ("st", 1), ("sb", 1), ("at", -1), ("sa",), ("at", 0),
+    ("yf", 1), ("st", 0), ("l", 0), ("fa",), ("fb",), ("yf", 0),
 )
 
 
@@ -52,12 +52,22 @@
         return (name, min(key[1], 1))
     if name in ("ar", "br"):
         return ("row", abs(key[1]))
-    if name in ("bx", "bxr"):
+    if name == "bx" and key[2] > 0:
+        return (name, abs(key[1]))
+    if name == "bx":
+        return ("bxr", abs(key[1]))
+    if name == "bxr":
         return (name, abs(key[1]))
     if name == "sx":
         return (name, abs(key[1]), key[2])
     if name == "y":
         return (name, key[1], 2 if key[2] == 2 else 1)
+    if name == "az" and key[2] == 3:
+        return ("az", 3)
+    if name == "sz" and key[2] == 1:
+        return ("sz", abs(key[1]))
+    if name in ("sz", "sa", "sb"):
+        return key[:-2]
     return key[:-1]
 
 
@@ -89,27 +99,42 @@
     yp = {k: at(z, x, c, yk(k)) for k in DIRS}
     pal = at(z, x, 1 - c, y)
 
-    local = []
-
-    def load(src, dst):
-        copy = pltpu.make_async_copy(src, dst, local_sem.at[len(local)])
-        copy.start()
-        local.append(copy)
-        return copy
-
-    stores = []
+    local = {}
+
+    def load(group, src, dst):
+        into = local.setdefault(group, [len(local), 0, False])
+        pltpu.make_async_copy(src, dst, local_sem.at[into[0]]).start()
+        into[1] += bytes_of(src)
+
+    def loaded(group):
+        into = local[group]
+        if not into[2]:
+            into[2] = True
+            taken(local_sem.at[into[0]], into[1])
+
+    def bytes_of(ref):
+        size = ref.dtype.itemsize
+        for extent in ref.shape:
+            size *= extent
+        return size
+
+    def taken(sem, size):
+        ref = sized.at[pl.ds(0, size // 512)]
+        pltpu.make_async_copy(ref, ref, sem).wait()
 
     def store(src, dst):
-        stores.append(load(src, dst))
-
-    in_w = [
-        load(w_up, w.at[z, x, c, :, pl.ds(HID, HID)]),
-        load(w_gate, w.at[z, x, c, :, pl.ds(0, HID)]),
-    ]
-    in_xe = [load(x_early.at[pl.ds(h * HALF, HALF)], xe.at[y, h]) for h in range(2)]
-    in_xl = [load(x_late.at[pl.ds(h * HALF, HALF)], xl.at[y, h]) for h in range(2)]
-    in_dh = [load(d_hidden.at[pl.ds(i * ROWS, ROWS)], dh.at[i]) for i in range(Y)]
-    in_sums = [load(gate_sum, sums.at[:, pl.ds(0, HID)]), load(up_sum, sums.at[:, pl.ds(HID, HID)])]
+        load("out", src, dst)
+
+    load("w", w_up, w.at[z, x, c, :, pl.ds(HID, HID)])
+    load("w", w_gate, w.at[z, x, c, :, pl.ds(0, HID)])
+    for h in range(2):
+        load("xe", x_early.at[pl.ds(h * HALF, HALF)], xe.at[y, h])
+    for h in range(2):
+        load("xl", x_late.at[pl.ds(h * HALF, HALF)], xl.at[y, h])
+    for i in range(Y):
+        load("rest", d_hidden.at[pl.ds(i * ROWS, ROWS)], dh.at[i])
+    load("rest", gate_sum, sums.at[:, pl.ds(0, HID)])
+    load("rest", up_sum, sums.at[:, pl.ds(HID, HID)])
 
     with jax.named_scope("entry"):
         barrier = pltpu.get_barrier_semaphore()
@@ -118,10 +143,6 @@
         pl.semaphore_wait(barrier, 7)
 
     groups, links = {}, {}
-
-    def taken(sem, size):
-        ref = sized.at[pl.ds(0, size // 512)]
-        pltpu.make_async_copy(ref, ref, sem).wait()
 
     def send(key, src, dst, peer):
         group, link = group_of(key), id(peer)
@@ -133,11 +154,8 @@
             src_ref=src, dst_ref=dst, send_sem=send_sem.at[out[0]], recv_sem=recv_sem.at[into[0]],
             device_id=peer, device_id_type=MESH,
         ).start()
-        size = src.dtype.itemsize
-        for extent in src.shape:
-            size *= extent
-        into[1] += size
-        out[1] += size
+        into[1] += bytes_of(src)
+        out[1] += bytes_of(src)
 
     def push(key, ref, peer):
         send(key, ref, ref, peer)
@@ -155,18 +173,18 @@
     CA, CB = pl.ds(0, NA), pl.ds(NA, NB)
 
     def own():
-        for copy in in_w:
-            copy.wait()
-        for k in DIRS:
-            push(("bz", 0, k), w.at[z, x, c, :, CB], zp[k])
+        loaded("w")
+        for p in (1, -1):
+            for k in DIRS:
+                push(("bz", 0, p, k), w.at[z, x, c, half(p * k), CB], zp[k])
         for k in DIRS:
             push(("ax", k), w.at[z, x, c, :, CA], xp[k])
-        for k in DIRS:
-            push(("bx", 0, k), w.at[z, x, c, :, CB], xp[k])
+        for p in (1, -1):
+            for k in DIRS:
+                push(("bx", 0, p, k), w.at[z, x, c, half(p * k), CB], xp[k])
         for k in DIRS:
             push(("az", 0, 0, k), w.at[z, x, c, :, CA], zp[k])
-        for copy in in_xe:
-            copy.wait()
+        loaded("xe")
         y_own("xe", xe)
 
     def y_own(name, ref):
@@ -181,8 +199,7 @@
             push((name, 2, k), ref.at[yk(-k), 0 if k > 0 else 1], yp[k])
 
     def xl_own():
-        for copy in in_xl:
-            copy.wait()
+        loaded("xl")
         y_own("xl", xl)
 
     def turn(block):
@@ -223,6 +240,8 @@
             push(("az", 2, 0, k), w.at[z, xk(2), c, :, CA], zp[k])
 
     def az(j, n):
+        if n == 4:
+            return
         wait("az", j, n - 1)
         if n < 4:
             for k in DIRS:
@@ -230,21 +249,24 @@
                 push(("az", j, n, k), w.at[zk(-k * n), xk(j), c, rows, CA], zp[k])
 
     def ar(n):
+        if n == 4:
+            wait("az", 3)
         for r in rows_of(n):
             push(("ar", r), w.at[zk(r), :, c, :, CA], pal)
 
-    def bz(n):
-        wait("bz", n - 1)
+    def bz(n, p):
+        wait("bz", n - 1, p)
+        for k in DIRS:
+            push(("bz", n, p, k), w.at[zk(-k * n), x, c, half(p * k), CB], zp[k])
+
+    def bzx(n):
+        wait("bz", n - 1, 1)
         if n < 4:
-            for k in DIRS:
-                rows = half(k) if n == 3 else ALL
-                push(("bz", n, k), w.at[zk(-k * n), x, c, rows, CB], zp[k])
-
-    def bzx(n):
-        wait("bz", n - 1)
-        for r in rows_of(n):
-            for k in DIRS:
-                push(("bx", r, k), w.at[zk(r), x, c, :, CB], xp[k])
+            wait("bz", n - 1, -1)
+        for p in (1, -1):
+            for r in rows_of(n):
+                for k in DIRS:
+                    push(("bx", r, p, k), w.at[zk(r), x, c, half(p * k), CB], xp[k])
 
     def bx(n):
         wait("bx", n)
@@ -274,8 +296,7 @@
             acc[block] = piece if n == 0 else acc[block] + piece
 
     def f2():
-        for copy in (*in_dh, *in_sums):
-            copy.wait()
+        loaded("rest")
         for block, piece in rows_product((0, 1, -1, 2, -2), (2,)):
             acc[block] = piece
 
@@ -306,17 +327,17 @@
     def slot(kind, key):
         return slots.setdefault((kind, key), sum(1 for name in slots if name[0] == kind))
 
-    def sent(kind, key, value, peer, rows=ALL, more=None, more_rows=None):
+    def sent(kind, key, value, peer, rows=ALL, more=None, more_rows=None, part=0):
         stage, into = (a_stage, a_in) if kind == "a" else (b_stage, b_in)
         i = slot(kind, key)
         stage[i, rows] = value.astype(BF16)
         if more is not None:
             stage[i, more_rows] = more.astype(BF16)
             rows = ALL
-        send(key, stage.at[i, rows], into.at[i, rows], peer)
+        send((*key, part), stage.at[i, rows], into.at[i, rows], peer)
 
     def came(kind, *key):
-        wait(*group_of(key))
+        wait(*group_of((*key, 0)))
         ref = a_in if kind == "a" else b_in
         return ref, slot(kind, key)
 
@@ -333,6 +354,9 @@
         for r in rows:
             for k in DIRS:
                 sent("b", ("sx", r, 2, k), s[zk(r), xk(2), half(k), CB], xp[k], half(k))
+        for r in rows:
+            for k in DIRS:
+                sent("b", ("sx", r, 1, k), s[zk(r), xk(k), half(-k), CB], xp[k], half(-k), part=1)
         if n == 4:
             for j in (2, 1, -1, 0):
                 for k in DIRS:
@@ -340,6 +364,9 @@
 
     def onward(kind, before, key, own, peer, partly, k):
         ref, i = came(kind, *before)
+        if partly is None:
+            sent(kind, key, own(half(k)) + ref[i, half(k)].astype(F32), peer, half(k))
+            return
         if partly:
             mine, rest = half(k), half(-k)
             sent(kind, key, own(mine) + ref[i, mine].astype(F32), peer, mine, own(rest), rest)
@@ -349,7 +376,7 @@
     def sx(n):
         for r in rows_of(n):
             for k in DIRS:
-                onward("b", ("sx", r, 2, k), ("sx", r, 1, k), lambda q: s[zk(r), xk(k), q, CB], xp[k], True, k)
+                onward("b", ("sx", r, 2, k), ("sx", r, 1, k), lambda q: s[zk(r), xk(k), q, CB], xp[k], None, k)
 
     def both(kind, own, *key):
         value = own
@@ -434,11 +461,12 @@
     for name, *args in ORDER:
         with jax.named_scope("_".join(map(str, (name, *args)))):
             tasks[name](*args)
+    if len(groups) != GROUPS:
+        raise ValueError(len(groups))
     with jax.named_scope("drain"):
         for i, size in links.values():
             taken(send_sem.at[i], size)
-        for copy in stores:
-            copy.wait()
+        loaded("out")
 
 
 def finish(*refs):
@@ -488,7 +516,7 @@
                 vmem((SIZED, 128), F32),
                 pltpu.SemaphoreType.DMA((7,)),
                 pltpu.SemaphoreType.DMA((GROUPS,)),
-                pltpu.SemaphoreType.DMA((20,)),
+                pltpu.SemaphoreType.DMA((5,)),
             ],
             compiler_params=pltpu.CompilerParams(
                 collective_id=0, has_side_effects=True, vmem_limit_bytes=VMEM_MIB * 1024 * 1024

time: 66.3 us -> 64.7 us (0.976)
  Pallas kernels: 65.5 us -> 64 us
    pallas_call x1, Pallas kernels: 63.2 us -> 61.6 us  [local(): pl.pallas_call(kernel, out_shape=OUTS, in_specs=[any_space] * 7, out_spec...]
where the time goes in v5:
time: 64.7 us; the launch traced here: 64.6 us
  Pallas kernels  64 us (99%)
    pallas_call x1, Pallas kernels, local(): pl.pallas_call(kernel, out_shape=OUTS, in_specs=[any_space] * 7, out_spec...  61.6 us
    pallas_call x1, Pallas kernels, local(): pl.pallas_call(finish, out_shape=OUTS, in_specs=[any_space] * 4, out_spec...  2.31 us

profile of v5, /device:TPU:2, one launch (start us, length us, event | category | flops | bytes accessed | tf_op | source)
XLA Modules:
  0.0 64.6 jit_solution(5390734383223659120)
XLA Ops:
  0.6 61.6 %layer.1 = (bf16[512,768]{1,0:T(8,128)(2,1)}, bf16[128,2048]{1,0:T(8,128)(2,1)}, f32[32,768]{1,0:T(8,128)}, f32[32,768]{1,0:T(8,128)}) custom-call(bf16[128,2048]{1,0:T(8,128)(2,1)} %x_late.1, bf16[128,2048]{1,0:T(8,128)(2,1)} %x_early.1, bf16[512,768]{1,0:T(8,128)(2,1)} %d_hidden.1, bf16[32,768]{1,0:T(8,128)(2,1)} %w_gate.1, bf16[32,768]{1,0:T(8,128)(2,1)} %w_up.1, ...), custom_call_target="tpu_custom_call" | custom-call | flops 12884901888 | bytes 8388608 | tf_op jit(solution)/shard_map/layer/pallas_call | solution.py:488
  62.3 2.3 %finish.1 = (bf16[512,768]{1,0:T(8,128)(2,1)}, bf16[128,2048]{1,0:T(8,128)(2,1)}, f32[32,768]{1,0:T(8,128)}, f32[32,768]{1,0:T(8,128)}) custom-call(bf16[512,768]{1,0:T(8,128)(2,1)} %get-tuple-element.8.refs_0_, bf16[128,2048]{1,0:T(8,128)(2,1)} %get-tuple-element.9.refs_1_, f32[32,768]{1,0:T(8,128)} %get-tuple-element.10.refs_2_, ...), custom_call_target="tpu_custom_call" | custom-call | tf_op jit(solution)/shard_map/finish/pallas_call | solution.py:528

commit v6 on v5

--- a/solution.py
+++ b/solution.py
@@ -16,7 +16,7 @@
 MESH = pl.DeviceIdType.MESH
 F32, BF16 = jnp.float32, jnp.bfloat16
 DIRS = (1, -1)
-GROUPS, SIZED = 79, 11264
+GROUPS, SIZED = 78, 11264
 ORDER = (
     ("own",), ("bz", 1, 1), ("ax1",), ("bz", 1, -1), ("bx", 0), ("bzx", 1), ("az0",), ("t", 0), ("az", 0, 1),
     ("bz", 2, 1), ("ax2",), ("bzx", 2), ("bz", 2, -1), ("bx", 1), ("br", 0), ("ar", 0), ("xer",),
@@ -29,8 +29,8 @@
     ("sx", 3), ("sz", 0, 3), ("i", 1), ("st", 4), ("sz", 2, 2), ("w", 1), ("sz", 1, 2), ("i", 0),
     ("sz", -1, 2), ("y1", 0), ("sx", 2), ("sz", 0, 2), ("y2", 1), ("st", 3), ("sb", 3), ("sz", 2, 1),
     ("l", 1), ("w", 0), ("sz", -1, 1), ("sz", 1, 1), ("l", 2), ("sx", 1), ("st", 2), ("sb", 2), ("at", 2),
-    ("sz", 0, 1), ("y2", 0), ("at", 1), ("sx", 0), ("st", 1), ("sb", 1), ("at", -1), ("sa",), ("at", 0),
-    ("yf", 1), ("st", 0), ("l", 0), ("fa",), ("fb",), ("yf", 0),
+    ("sz", 0, 1), ("y2", 0), ("sx", 0), ("l", 0), ("at", 1), ("st", 1), ("sb", 1), ("at", -1), ("sa",),
+    ("at", 0), ("yf", 1), ("st", 0), ("fa",), ("fb",), ("yf", 0),
 )
 
 
@@ -45,7 +45,7 @@
 def group_of(key):
     name = key[0]
     if name in ("xt", "d"):
-        return (name,)
+        return ("d",)
     if name == "xe":
         return (name, key[1])
     if name == "xl":
@@ -344,7 +344,6 @@
     def wgrad(n):
         if n == 4:
             wait("d")
-            wait("xt")
         rows = rows_of(n)
         mine = jnp.concatenate([xt[zk(r), :, c].reshape(X * SHARD, TOK) for r in rows], axis=0)
         theirs = jnp.concatenate([xtp[zk(r)].reshape(X * SHARD, TOK) for r in rows], axis=0)

time: 64.7 us -> 64.7 us (level)
  no operation moved by 1% of the time
where the time goes in v6:
time: 64.7 us; the launch traced here: 64.6 us
  Pallas kernels  63.9 us (99%)
    pallas_call x1, Pallas kernels, local(): pl.pallas_call(kernel, out_shape=OUTS, in_specs=[any_space] * 7, out_spec...  61.6 us
    pallas_call x1, Pallas kernels, local(): pl.pallas_call(finish, out_shape=OUTS, in_specs=[any_space] * 4, out_spec...  2.31 us

profile of v6, /device:TPU:2, one launch (start us, length us, event | category | flops | bytes accessed | tf_op | source)
XLA Modules:
  0.0 64.6 jit_solution(13450363532274078763)
XLA Ops:
  0.6 61.6 %layer.1 = (bf16[512,768]{1,0:T(8,128)(2,1)}, bf16[128,2048]{1,0:T(8,128)(2,1)}, f32[32,768]{1,0:T(8,128)}, f32[32,768]{1,0:T(8,128)}) custom-call(bf16[128,2048]{1,0:T(8,128)(2,1)} %x_late.1, bf16[128,2048]{1,0:T(8,128)(2,1)} %x_early.1, bf16[512,768]{1,0:T(8,128)(2,1)} %d_hidden.1, bf16[32,768]{1,0:T(8,128)(2,1)} %w_gate.1, bf16[32,768]{1,0:T(8,128)(2,1)} %w_up.1, ...), custom_call_target="tpu_custom_call" | custom-call | flops 12884901888 | bytes 8388608 | tf_op jit(solution)/shard_map/layer/pallas_call | solution.py:487
  62.3 2.3 %finish.1 = (bf16[512,768]{1,0:T(8,128)(2,1)}, bf16[128,2048]{1,0:T(8,128)(2,1)}, f32[32,768]{1,0:T(8,128)}, f32[32,768]{1,0:T(8,128)}) custom-call(bf16[512,768]{1,0:T(8,128)(2,1)} %get-tuple-element.8.refs_0_, bf16[128,2048]{1,0:T(8,128)(2,1)} %get-tuple-element.9.refs_1_, f32[32,768]{1,0:T(8,128)} %get-tuple-element.10.refs_2_, ...), custom_call_target="tpu_custom_call" | custom-call | tf_op jit(solution)/shard_map/finish/pallas_call | solution.py:527
